TPU v7x, 256 devices: a whole 4x4x8 slice. The times are simulated.
256 devices in a mesh: ep: 64 (over z, x, core), tp: 4 (over y).
Axes of the slice: x: 4, y: 4, z: 8, core: 2. Of those that a mesh axis runs over, the one named last changes fastest.
Arguments:
- query_rows: bfloat16 [16384, 1024], P('ep', 'tp'), may hold values from -8 to 8
- key_rows: bfloat16 [16384, 256], P('ep', 'tp'), may hold values from -8 to 8
- value_rows: bfloat16 [16384, 256], P('ep', 'tp'), may hold values from -16 to 16
- query_gain: float32 [64], replicated, may hold values from 0.5 to 7.5
- key_gain: float32 [64], replicated, may hold values from 0.5 to 7.5
- moe_tokens: bfloat16 [32768, 2048], P(('ep', 'tp')), may hold values from -6 to 6
- norm_gain: float32 [2048], replicated, may hold values from 0.1 to 1.9
- routes: int32 [32768, 2], P('ep'), may hold values from 0 to 63, all different within a row; in each aligned block of 128 rows (0 to 127, 128 to 255, ...) at most 8 rows name the same one
- route_weights: float32 [32768, 2], P('ep'), may hold values from 0.1 to 1
- expert_gate: bfloat16 [64, 2048, 1024], P('ep', None, 'tp'), may hold values from -0.125 to 0.125
- expert_up: bfloat16 [64, 2048, 1024], P('ep', None, 'tp'), may hold values from -0.125 to 0.125
- expert_down: bfloat16 [64, 1024, 2048], P('ep', 'tp'), may hold values from -0.1875 to 0.1875
- shared_gate: bfloat16 [2048, 1024], P(None, 'tp'), may hold values from -0.125 to 0.125
- shared_up: bfloat16 [2048, 1024], P(None, 'tp'), may hold values from -0.125 to 0.125
- shared_down: bfloat16 [1024, 2048], P('tp'), may hold values from -0.1875 to 0.1875
Outputs:
- attn_out: bfloat16 [16384, 1024], P('ep', 'tp')
- moe_out: bfloat16 [32768, 2048], P(('ep', 'tp'))
Inputs may be any that keep to these rules, and one draw needn't show every extreme that they name: `routes`: each row names 2 different experts. Within each aligned block of 128 rows no expert is named more than 8 times, and in every draw some expert is named exactly 8 times in some block.
All inputs are finite; a program needn't handle non-finite values.
Results may differ from a plain program's by a relative error of at most 0.012.
The roundings to bfloat16 on the way count: a program that leaves them out, or rounds other values in their place, can miss the bound.
Values may be sent and summed in bfloat16 or wider, within the bound.
No kernel may reach another device: no remote copies, remote signals or barrier semaphores. Data moves between devices by JAX's collectives and lax.ppermute only.
A program may use at most 192 MiB of HBM per device.

v0:
```python
import jax
import jax.numpy as jnp
from jax import lax
from jax.sharding import Mesh
from jax.sharding import PartitionSpec as P

GRID_W = 64
EP = ("ep_0", "ep_1", "ep_2")
EP_TP = ("ep_0", "ep_1", "ep_2", "tp")


epsilon = 1e-06
rotary_base = 10000.0
routed_scale = 2.5


def joined_along(pieces, dim):
    lengths = list(pieces.shape[1:])
    lengths[dim] *= pieces.shape[0]
    return jnp.moveaxis(pieces, 0, dim).reshape(lengths)


def stacked_from(array, axes, order):
    pieces = array
    for k in order:
        pieces = lax.all_gather(pieces, axes[k])
    done = order[::-1]
    back = [done.index(k) for k in range(len(axes))]
    pieces = pieces.transpose(*back, *range(len(axes), pieces.ndim))
    return pieces.reshape(-1, *array.shape)


def gathered_by_axis(array, axes, order, dim):
    return joined_along(stacked_from(array, axes, order), dim)


def copy_for_each(array, axis):
    count = lax.axis_size(axis)
    return lax.all_to_all(
        jnp.broadcast_to(array[None], (count, *array.shape)), axis, 0, 0, tiled=True
    )


def gathered_copies(array, axis, dim):
    pieces = copy_for_each(array, axis)
    return joined_along(pieces, dim)


def cut_along(array, dim, count):
    before, after = (array.shape[:dim], array.shape[dim + 1 :])
    return jnp.moveaxis(array.reshape(*before, count, -1, *after), dim, 0)


def sent_and_summed(array, axis, dim):
    pieces = cut_along(array, dim, lax.axis_size(axis))
    arrived = lax.all_to_all(pieces, axis, split_axis=0, concat_axis=0, tiled=True)
    return arrived.astype(jnp.float32).sum(axis=0)


def rotate_heads(heads_in, gain_row, positions):
    values32 = heads_in.astype(jnp.float32)
    scaled = (
        values32
        * lax.rsqrt(jnp.mean(values32 * values32, axis=-1, keepdims=True) + epsilon)
        * gain_row
    )
    pair_count = scaled.shape[-1] // 4
    inv_freq = rotary_base ** (-jnp.arange(pair_count, dtype=jnp.float32) / pair_count)
    grid_row = (positions // GRID_W).astype(jnp.float32)
    grid_col = (positions % GRID_W).astype(jnp.float32)
    angles = jnp.concatenate([grid_row[:, None] * inv_freq, grid_col[:, None] * inv_freq], axis=-1)[
        :, None, :
    ]
    cosine = jnp.cos(angles)
    sine_part = jnp.sin(angles)
    first_half = scaled[..., 0::2]
    second_half = scaled[..., 1::2]
    turned = jnp.stack(
        [
            first_half * cosine - second_half * sine_part,
            first_half * sine_part + second_half * cosine,
        ],
        axis=-1,
    )
    return turned.reshape(scaled.shape).astype(jnp.bfloat16)


def span_length(row_count):
    length = min(row_count, 2048)
    while row_count % length:
        length -= 1
    return length


def attend(query_rows, key_rows, value_rows, query_gain, key_gain):
    row_count = query_rows.shape[0]
    head_size = query_gain.shape[0]
    q_heads = query_rows.shape[1] // head_size
    kv_heads = key_rows.shape[1] // head_size
    group = q_heads // kv_heads
    scale = head_size ** (-0.5)
    positions = lax.axis_index(EP) * row_count + jnp.arange(row_count, dtype=jnp.int32)
    q_rot = rotate_heads(query_rows.reshape(row_count, q_heads, head_size), query_gain, positions)
    k_rot = rotate_heads(key_rows.reshape(row_count, kv_heads, head_size), key_gain, positions)
    key_value = jnp.stack([k_rot, value_rows.reshape(row_count, kv_heads, head_size)], axis=2)
    key_value = key_value.reshape(row_count, kv_heads * 2 * head_size)
    q_grouped = q_rot.reshape(row_count, kv_heads, group, head_size).transpose(1, 2, 0, 3)
    q_grouped = q_grouped.reshape(kv_heads, group * row_count, head_size)
    query_count = group * row_count
    initial = (
        jnp.full((kv_heads, query_count), -jnp.inf, jnp.float32),
        jnp.zeros((kv_heads, query_count), jnp.float32),
        jnp.zeros((kv_heads, query_count, head_size), jnp.float32),
    )

    def one_span(carried, span_rows):
        run_max, run_sum, mixed = carried
        keys_span = span_rows[:, :, 0, :]
        values_span = span_rows[:, :, 1, :]
        scores = (
            jnp.einsum("hrd,shd->hrs", q_grouped, keys_span, preferred_element_type=jnp.float32)
            * scale
        )
        new_max = jnp.maximum(run_max, jnp.max(scores, axis=-1))
        factor = jnp.exp(run_max - new_max)
        weights = jnp.exp(scores - new_max[..., None])
        run_sum = run_sum * factor + jnp.sum(weights, axis=-1)
        added = jnp.einsum(
            "hrs,shd->hrd",
            weights.astype(jnp.bfloat16),
            values_span,
            preferred_element_type=jnp.float32,
        )
        mixed = mixed * factor[..., None] + added
        return ((new_max, run_sum, mixed), None)

    carried = initial
    piece_rows = gathered_by_axis(key_value, (("ep_0", "ep_1"), "ep_2"), (0, 1), 0)
    piece_count = piece_rows.shape[0]
    length = span_length(piece_count)
    spans = piece_rows.reshape(piece_count // length, length, kv_heads, 2, head_size)
    carried, unused = lax.scan(one_span, carried, spans)
    run_max, run_sum, mixed = carried
    result = (mixed / run_sum[..., None]).astype(jnp.bfloat16)
    result = result.reshape(kv_heads, group, row_count, head_size).transpose(2, 0, 1, 3)
    return result.reshape(row_count, q_heads * head_size)


def slot_ranks(route_rows, tok_rows, experts):
    top_count = route_rows.shape[1]
    blocks = route_rows.shape[0] // tok_rows
    chosen = route_rows.reshape(blocks, tok_rows * top_count)
    one_hot = (chosen[:, :, None] == jnp.arange(experts, dtype=jnp.int32)[None, None, :]).astype(
        jnp.int32
    )
    ranks = jnp.sum((jnp.cumsum(one_hot, axis=1) - one_hot) * one_hot, axis=2)
    return (chosen, ranks)


def build_send(source, chosen, ranks, tok_rows, top_count, capacity, experts):
    blocks = chosen.shape[0]
    model_width = source.shape[1]
    block_ids = jnp.arange(blocks, dtype=jnp.int32)[:, None]
    dest = (chosen * blocks + block_ids) * capacity + ranks
    rows_from = (
        block_ids * tok_rows
        + jnp.arange(tok_rows * top_count, dtype=jnp.int32)[None, :] // top_count
    )
    slot_rows = jnp.full((experts * blocks * capacity,), blocks * tok_rows, jnp.int32)
    slot_rows = slot_rows.at[dest.reshape(-1)].set(rows_from.reshape(-1))
    padded = jnp.concatenate([source, jnp.zeros((1, model_width), source.dtype)], axis=0)
    return padded[slot_rows].reshape(experts, blocks * capacity, model_width)


def expert_products(arrived, w_gate, w_up, w_down):
    gate_proj = jnp.einsum("lrd,ldf->lrf", arrived, w_gate, preferred_element_type=jnp.float32)
    up_proj = jnp.einsum("lrd,ldf->lrf", arrived, w_up, preferred_element_type=jnp.float32)
    hidden = (jax.nn.silu(gate_proj) * up_proj).astype(jnp.bfloat16)
    return jnp.einsum("lrf,lfd->lrd", hidden, w_down, preferred_element_type=jnp.float32)


def shared_products(rows_in, w_gate, w_up, w_down):
    gate_proj = jnp.dot(rows_in, w_gate, preferred_element_type=jnp.float32)
    up_proj = jnp.dot(rows_in, w_up, preferred_element_type=jnp.float32)
    hidden = (jax.nn.silu(gate_proj) * up_proj).astype(jnp.bfloat16)
    return jnp.dot(hidden, w_down, preferred_element_type=jnp.float32)


def experts_half(
    moe_tokens,
    norm_gain,
    routes,
    route_weights,
    expert_gate,
    expert_up,
    expert_down,
    shared_gate,
    shared_up,
    shared_down,
):
    tok_rows, model_width = moe_tokens.shape
    top_count = routes.shape[1]
    tp_size = lax.axis_size("tp")
    ep_size = lax.axis_size(EP)
    local_experts = expert_gate.shape[0]
    experts = local_experts * ep_size
    capacity = 2 * tok_rows * top_count // experts
    lane = lax.axis_index("tp")
    values32 = moe_tokens.astype(jnp.float32)
    normed = (
        values32
        * lax.rsqrt(jnp.mean(values32 * values32, axis=-1, keepdims=True) + epsilon)
        * norm_gain
    ).astype(jnp.bfloat16)
    gates = route_weights / jnp.sum(route_weights, axis=-1, keepdims=True) * routed_scale
    own_gates = lax.dynamic_slice_in_dim(gates, lane * tok_rows, tok_rows, 0)
    group_rows = gathered_copies(normed.reshape(1, 1, 1, tok_rows, model_width), "tp", 2)
    chosen, ranks = slot_ranks(routes, tok_rows, experts)
    send = build_send(
        group_rows.reshape(tp_size * tok_rows, model_width),
        chosen,
        ranks,
        tok_rows,
        top_count,
        capacity,
        experts,
    )
    arrived = lax.all_to_all(send, EP, split_axis=0, concat_axis=1, tiled=True)
    own_chosen = lax.dynamic_index_in_dim(chosen, lane, 0, keepdims=False)
    own_ranks = lax.dynamic_index_in_dim(ranks, lane, 0, keepdims=False)
    routed_part = expert_products(arrived, expert_gate, expert_up, expert_down)
    shared_part = shared_products(
        group_rows.reshape(tp_size * tok_rows, model_width), shared_gate, shared_up, shared_down
    )
    routed_sum, shared_sum = (
        sent_and_summed(
            routed_part.reshape(local_experts, ep_size, tp_size, capacity, model_width).astype(
                jnp.bfloat16
            ),
            "tp",
            2,
        ),
        sent_and_summed(
            shared_part.reshape(1, 1, tp_size, tok_rows, model_width).astype(jnp.bfloat16), "tp", 2
        ),
    )
    outgoing = routed_sum.astype(jnp.bfloat16).reshape(
        local_experts, ep_size * capacity, model_width
    )
    returned = lax.all_to_all(outgoing, EP, split_axis=1, concat_axis=0, tiled=True)
    flat_rows = returned.reshape(experts * capacity, model_width)
    picked = flat_rows[own_chosen * capacity + own_ranks].reshape(tok_rows, top_count, model_width)
    routed_total = jnp.sum(own_gates[:, :, None] * picked.astype(jnp.float32), axis=1)
    return (routed_total + shared_sum.reshape(tok_rows, model_width)).astype(jnp.bfloat16)


def body(
    query_rows,
    key_rows,
    value_rows,
    query_gain,
    key_gain,
    moe_tokens,
    norm_gain,
    routes,
    route_weights,
    expert_gate,
    expert_up,
    expert_down,
    shared_gate,
    shared_up,
    shared_down,
):
    attn_out = attend(query_rows, key_rows, value_rows, query_gain, key_gain)
    moe_out = experts_half(
        moe_tokens,
        norm_gain,
        routes,
        route_weights,
        expert_gate,
        expert_up,
        expert_down,
        shared_gate,
        shared_up,
        shared_down,
    )
    return (attn_out, moe_out)


def solution(mesh):
    finer = Mesh(mesh.devices.reshape(8, 4, 2, mesh.shape["tp"]), ("ep_0", "ep_1", "ep_2", "tp"))
    return jax.shard_map(
        body,
        mesh=finer,
        in_specs=(
            P(EP, "tp"),
            P(EP, "tp"),
            P(EP, "tp"),
            P(),
            P(),
            P(EP_TP, None),
            P(),
            P(EP, None),
            P(EP, None),
            P(EP, None, "tp"),
            P(EP, None, "tp"),
            P(EP, "tp", None),
            P(None, "tp"),
            P(None, "tp"),
            P("tp", None),
        ),
        out_specs=(P(EP, "tp"), P(EP_TP, None)),
        check_vma=False,
    )
```

profile of v0, /device:TPU:2, one launch (start us, length us, event | category | flops | bytes accessed | tf_op | source)
XLA Modules:
  0.0 510.0 jit_solution(16651082673510238095)
XLA Ops:
  9.8 1.6 broadcast_in_dim.15
  11.4 4.5 all-to-all-start
  17.5 4.5 reduce-window.6
  24.2 4.3 scatter_custom_fusion
  28.5 13.7 %all-to-all-done = bf16[4,1,1,1,128,2048]{5,4,3,2,1,0:T(8,128)(2,1)S(1)} async-done(((bf16[4,1,1,1,128,2048]{5,4,3,2,1,0:T(8,128)(2,1)}), bf16[4,1,1,1,128,2048]{5,4,3,2,1,0:T(8,128)(2,1)S(1)}, u32[]{:S(2)}, u32[]{:S(2)}) %all-to-all-start) | async-done | bytes 2097184 | tf_op jit(solution)/shard_map/all_to_all | solution.py:39
  43.5 1.7 concatenate.33
  45.3 11.0 %gather_fusion = bf16[2048,2048]{1,0:T(8,128)(2,1)} fusion(bf16[513,2048]{1,0:T(8,128)(2,1)S(1)} %concatenate.33, s32[2048]{0:T(1024)S(1)} %fusion.48), kind=kCustom, calls=%fused_computation | custom fusion | bytes 16785408 | tf_op jit(solution)/shard_map/gather | solution.py:172
  56.3 12.3 %all-to-all-start.1 = ((bf16[64,32,2048]{2,1,0:T(8,128)(2,1)}), bf16[64,32,2048]{2,1,0:T(8,128)(2,1)}, u32[]{:S(2)}, u32[]{:S(2)}) async-start(bf16[64,32,2048]{2,1,0:T(8,128)(2,1)} %bitcast.157), calls=%async_computation.1 | async-start | bytes 16777216 | tf_op jit(solution)/shard_map/all_to_all | solution.py:228
  70.0 2.7 fusion.60
  72.8 5.4 %convolution_convert_fusion = bf16[512,2048]{1,0:T(8,128)(2,1)} fusion(bf16[256,2048]{1,0:T(8,128)(2,1)} %param.31, bf16[512,2048]{1,0:T(8,128)(2,1)S(1)} %bitcast.163, bf16[2048,256]{1,0:T(8,128)(2,1)} %param.30, f32[512,256]{1,0:T(8,128)} %fusion.60), kind=kOutput, calls=%fused_computation.25 | convolution fusion | flops 1075576832 | bytes 6815744 | tf_op jit(solution)/shard_map/dot_general | solution.py:186
  78.1 189.1 %all-to-all-done.1 = bf16[64,32,2048]{2,1,0:T(8,128)(2,1)} async-done(((bf16[64,32,2048]{2,1,0:T(8,128)(2,1)}), bf16[64,32,2048]{2,1,0:T(8,128)(2,1)}, u32[]{:S(2)}, u32[]{:S(2)}) %all-to-all-start.1) | async-done | bytes 8388640 | tf_op jit(solution)/shard_map/all_to_all | solution.py:228
  267.2 3.8 all-to-all-start.4
  271.0 6.0 %fusion.23 = f32[2048,256]{1,0:T(8,128)S(1)} fusion(bf16[2048,2048]{1,0:T(8,128)(2,1)} %bitcast.24, bf16[1,2048,256]{2,1,0:T(8,128)(2,1)} %param.26), kind=kOutput, calls=%fused_computation.39 | convolution fusion | flops 2147483648 | bytes 11534336 | tf_op jit(solution)/shard_map/lrd,ldf->lrf/dot_general | solution.py:176
  277.0 6.0 %fusion.16 = bf16[2048,256]{1,0:T(8,128)(2,1)S(1)} fusion(bf16[2048,2048]{1,0:T(8,128)(2,1)} %bitcast.24, f32[2048,256]{1,0:T(8,128)S(1)} %fusion.23, bf16[1,2048,256]{2,1,0:T(8,128)(2,1)S(1)} %copy-done.11), kind=kOutput, calls=%fused_computation.27 | convolution fusion | flops 2150629376 | bytes 12582912 | tf_op jit(solution)/shard_map/lrd,ldf->lrf/dot_general | solution.py:177
  283.1 5.5 %convert_bitcast_fusion = bf16[4,1,64,1,8,2048]{5,4,0,2,3,1:T(8,128)(2,1)} fusion(bf16[64,4,8,256]{3,2,1,0:T(8,128)(2,1)S(1)} %bitcast.169, bf16[1,256,2048]{2,1,0:T(8,128)(2,1)S(1)} %copy-done), kind=kOutput, calls=%fused_computation.23 | convolution fusion | flops 2151677952 | bytes 10485760 | tf_op jit(solution)/shard_map/lrf,lfd->lrd/dot_general | solution.py:179
  288.6 8.3 %copy.87 = bf16[4,1,64,1,8,2048]{5,4,2,3,1,0:T(8,128)(2,1)} copy(bf16[4,1,64,1,8,2048]{5,4,0,2,3,1:T(8,128)(2,1)} %convert_bitcast_fusion) | data formatting | bytes 16777216 | tf_op jit(solution)/shard_map/transpose | solution.py:51
  296.9 5.8 %all-to-all-start.2 = ((bf16[4,1,64,1,8,2048]{5,4,2,3,1,0:T(8,128)(2,1)}), bf16[4,1,64,1,8,2048]{5,4,2,3,1,0:T(8,128)(2,1)}, u32[]{:S(2)}, u32[]{:S(2)}) async-start(bf16[4,1,64,1,8,2048]{5,4,2,3,1,0:T(8,128)(2,1)} %copy.87), calls=%async_computation.2 | async-start | bytes 16777216 | tf_op jit(solution)/shard_map/all_to_all | solution.py:56
  304.7 1.4 convert_reduce_fusion
  306.1 16.2 %all-gather.6.cloned.1.call-done = bf16[64,256,128]{2,1,0:T(8,128)(2,1)} async-done(((bf16[32,256,128]{2,1,0:T(8,128)(2,1)}), bf16[64,256,128]{2,1,0:T(8,128)(2,1)}) %all-gather.6.cloned.1.call-update) | async-done | bytes 4194320 | tf_op jit(solution)/shard_map/all_gather | solution.py:26
  322.4 11.5 %copy.74 = bf16[32,2,256,128]{2,1,0,3:T(2,128)(2,1)} copy(bf16[32,2,256,128]{3,2,0,1:T(8,128)(2,1)} %bitcast.165) | data formatting | bytes 8388608 | tf_op jit(solution)/shard_map/transpose | solution.py:29
  333.8 7.9 %reshape_reshape_reshape.3 = bf16[8,2048,1,2,64]{1,0,4,3,2:T(8,128)(2,1)} reshape(bf16[32,2,256,128]{2,1,0,3:T(2,128)(2,1)} %copy.74) | data formatting | bytes 8388608 | tf_op jit(solution)/shard_map/reshape;reshape;reshape | solution.py:141
  341.7 6.4 %copy.77 = bf16[8,2048,1,2,64]{1,4,3,2,0:T(8,128)(2,1)} copy(bf16[8,2048,1,2,64]{1,0,4,3,2:T(8,128)(2,1)} %reshape_reshape_reshape.3) | data formatting | bytes 8388608
  348.1 47.6 %all-to-all-done.2 = bf16[4,1,64,1,8,2048]{5,4,2,3,1,0:T(8,128)(2,1)} async-done(((bf16[4,1,64,1,8,2048]{5,4,2,3,1,0:T(8,128)(2,1)}), bf16[4,1,64,1,8,2048]{5,4,2,3,1,0:T(8,128)(2,1)}, u32[]{:S(2)}, u32[]{:S(2)}) %all-to-all-start.2) | async-done | bytes 8388640 | tf_op jit(solution)/shard_map/all_to_all | solution.py:56
  395.6 5.7 %reduce_sum.94 = bf16[64,8,2048]{2,1,0:T(8,128)(2,1)S(1)} reduce(bf16[4,1,64,1,8,2048]{5,4,2,3,1,0:T(8,128)(2,1)} %all-to-all-done.2, bf16[]{:T(256)} %constant.138.clone.1), dimensions={0,1,3}, to_apply=%region_12.13 | reduce | flops 3145728 | bytes 10485762 | tf_op jit(solution)/shard_map/reduce_sum | solution.py:57
  401.3 5.2 %copy.102 = bf16[1,512,2048]{2,0,1:T(2,128)(2,1)} copy(bf16[1,512,2048]{2,1,0:T(8,128)(2,1)S(1)} %bitcast.164) | data formatting | bytes 4194304 | tf_op jit(solution)/shard_map/reshape | solution.py:247
  407.0 13.2 %reduce.11 = bf16[512,2048]{1,0:T(8,128)(2,1)S(1)} reduce(bf16[512,1,2048]{2,1,0:T(2,128)(2,1)} %bitcast.158, bf16[]{:T(256)} %broadcast.392), dimensions={1}, to_apply=%bitcast.136.reduce_sub_computation | reduce | bytes 4194306
  420.2 3.3 reshape.559
  423.4 7.7 %all-to-all-start.3 = ((bf16[64,2,8192]{2,1,0:T(2,128)(2,1)}), bf16[64,2,8192]{2,1,0:T(2,128)(2,1)S(1)}, u32[]{:S(2)}, u32[]{:S(2)}) async-start(bf16[64,2,8192]{2,1,0:T(2,128)(2,1)} %reshape.559), calls=%async_computation.3 | async-start | bytes 4194304 | tf_op jit(solution)/shard_map/all_to_all | solution.py:250
  431.1 43.8 %while.15 = (s32[]{:T(128)}, f32[1,1024]{1,0:T(1,128)S(1)}, f32[1,1024]{1,0:T(1,128)S(1)}, f32[1,1024,64]{1,2,0:T(8,128)S(1)}, bf16[8,2048,1,2,64]{1,4,3,2,0:T(8...) while((s32[]{:T(128)}, f32[1,1024]{1,0:T(1,128)S(1)}, ...), condition=%wide.region_5.6_spmd.clone, body=%wide.region_2.5_spmd.clone.sunk | while | flops 553849856 | bytes 27590764 | solution.py:142
  433.6 1.4 fusion.76
  435.0 1.6 fusion.78
  439.1 1.4 fusion.76
  440.5 1.6 fusion.78
  444.5 1.4 fusion.76
  446.0 1.6 fusion.78
  450.0 1.4 fusion.76
  451.5 1.6 fusion.78
  456.9 1.6 fusion.78
  462.4 1.6 fusion.78
  467.9 1.6 fusion.78
  473.4 1.6 fusion.78
  475.8 6.5 %all-to-all-done.3 = bf16[64,2,8192]{2,1,0:T(2,128)(2,1)S(1)} async-done(((bf16[64,2,8192]{2,1,0:T(2,128)(2,1)}), bf16[64,2,8192]{2,1,0:T(2,128)(2,1)S(1)}, u32[]{:S(2)}, u32[]{:S(2)}) %all-to-all-start.3) | async-done | bytes 2097184 | tf_op jit(solution)/shard_map/all_to_all | solution.py:250
  482.4 6.8 %reshape.560 = bf16[512,1,2048]{2,1,0:T(2,128)(2,1)} reshape(bf16[64,2,8192]{2,1,0:T(2,128)(2,1)S(1)} %all-to-all-done.3) | data formatting | bytes 4194304
  489.2 3.5 copy.101
  492.6 2.3 gather_fusion.1
  495.0 2.4 reshape.526
  497.4 3.2 multiply_reduce_fusion.1
  500.5 2.2 add_convert_fusion
  (138 shorter events, 37.3 us)
Async XLA Ops:
  7.2 275.9 %copy-start = (bf16[1,256,2048]{2,1,0:T(8,128)(2,1)S(1)}, bf16[1,256,2048]{2,1,0:T(8,128)(2,1)}, u32[]{:S(2)}) copy-start(bf16[1,256,2048]{2,1,0:T(8,128)(2,1)} %param.28) | copy-start | bytes 3145732
  7.2 8.7 %copy-start.7 = (s32[512,2]{0,1:T(2,128)S(1)}, s32[512,2]{0,1:T(2,128)}, u32[]{:S(2)}) copy-start(s32[512,2]{0,1:T(2,128)} %param.24) | copy-start | bytes 12292
  11.4 30.8 %all-to-all-start = ((bf16[4,1,1,1,128,2048]{5,4,3,2,1,0:T(8,128)(2,1)}), bf16[4,1,1,1,128,2048]{5,4,3,2,1,0:T(8,128)(2,1)S(1)}, u32[]{:S(2)}, u32[]{:S(2)}) async-start(bf16[4,1,1,1,128,2048]{5,4,3,2,1,0:T(8,128)(2,1)} %broadcast_in_dim.15), calls=%async_computation | async-start | bytes 4194304 | tf_op jit(solution)/shard_map/all_to_all | solution.py:39
  42.2 1.4 copy-start.2
  56.3 12.4 %copy-start.4 = (bf16[256,64]{0,1:T(8,128)(2,1)S(1)}, bf16[256,64]{0,1:T(8,128)(2,1)}, u32[]{:S(2)}) copy-start(bf16[256,64]{0,1:T(8,128)(2,1)} %param.18) | copy-start | bytes 98308
  56.3 12.5 %copy-start.9 = (f32[64]{0:T(128)S(1)}, f32[64]{0:T(128)}, u32[]{:S(2)}) copy-start(f32[64]{0:T(128)} %param.21) | copy-start | bytes 772
  56.3 12.9 %copy-start.6 = (bf16[256,64]{0,1:T(8,128)(2,1)S(1)}, bf16[256,64]{0,1:T(8,128)(2,1)}, u32[]{:S(2)}) copy-start(bf16[256,64]{0,1:T(8,128)(2,1)} %param.19) | copy-start | bytes 98308
  56.3 13.7 %copy-start.3 = (bf16[4,1,1,1,128,2048]{5,4,3,2,1,0:T(8,128)(2,1)S(1)}, bf16[4,1,1,1,128,2048]{5,4,3,2,1,0:T(8,128)(2,1)}, u32[]{:S(2)}) copy-start(bf16[4,1,1,1,128,2048]{5,4,3,2,1,0:T(8,128)(2,1)} %copy-done.2) | copy-start | bytes 6291460
  56.3 210.9 %all-to-all-start.1 = ((bf16[64,32,2048]{2,1,0:T(8,128)(2,1)}), bf16[64,32,2048]{2,1,0:T(8,128)(2,1)}, u32[]{:S(2)}, u32[]{:S(2)}) async-start(bf16[64,32,2048]{2,1,0:T(8,128)(2,1)} %bitcast.157), calls=%async_computation.1 | async-start | bytes 16777216 | tf_op jit(solution)/shard_map/all_to_all | solution.py:228
  68.7 234.1 %all-gather.4.cloned.1.call-start = ((), (), s32[]{:S(2)}) async-start(), calls=%async_computation.5 | async-start | bytes 2162688 | tf_op jit(solution)/shard_map/all_gather | solution.py:26
  267.2 29.7 %all-to-all-start.4 = ((bf16[4,1,1,1,128,2048]{5,4,3,2,1,0:T(8,128)(2,1)}), bf16[4,1,1,1,128,2048]{5,4,3,2,1,0:T(8,128)(2,1)S(1)}, u32[]{:S(2)}, u32[]{:S(2)}) async-start(bf16[4,1,1,1,128,2048]{5,4,3,2,1,0:T(8,128)(2,1)} %bitcast.168), calls=%async_computation.4 | async-start | bytes 4194304 | tf_op jit(solution)/shard_map/all_to_all | solution.py:56
  271.0 6.1 %copy-start.11 = (bf16[1,2048,256]{2,1,0:T(8,128)(2,1)S(1)}, bf16[1,2048,256]{2,1,0:T(8,128)(2,1)}, u32[]{:S(2)}) copy-start(bf16[1,2048,256]{2,1,0:T(8,128)(2,1)} %param.27) | copy-start | bytes 3145732
  296.9 6.6 %copy-start.5 = (bf16[256,256]{1,0:T(8,128)(2,1)S(1)}, bf16[256,256]{1,0:T(8,128)(2,1)}, u32[]{:S(2)}) copy-start(bf16[256,256]{1,0:T(8,128)(2,1)} %param.17) | copy-start | bytes 393220
  296.9 6.8 %copy-start.10 = (f32[64]{0:T(128)S(1)}, f32[64]{0:T(128)}, u32[]{:S(2)}) copy-start(f32[64]{0:T(128)} %param.20) | copy-start | bytes 772
  296.9 7.0 %copy-start.8 = (f32[512,2]{0,1:T(2,128)S(1)}, f32[512,2]{0,1:T(2,128)}, u32[]{:S(2)}) copy-start(f32[512,2]{0,1:T(2,128)} %param.25) | copy-start | bytes 12292
  296.9 98.8 %all-to-all-start.2 = ((bf16[4,1,64,1,8,2048]{5,4,2,3,1,0:T(8,128)(2,1)}), bf16[4,1,64,1,8,2048]{5,4,2,3,1,0:T(8,128)(2,1)}, u32[]{:S(2)}, u32[]{:S(2)}) async-start(bf16[4,1,64,1,8,2048]{5,4,2,3,1,0:T(8,128)(2,1)} %copy.87), calls=%async_computation.2 | async-start | bytes 16777216 | tf_op jit(solution)/shard_map/all_to_all | solution.py:56
  302.7 19.6 %all-gather.6.cloned.1.call-start = ((), (), s32[]{:S(2)}) async-start(), calls=%async_computation.6 | async-start | bytes 6291456 | tf_op jit(solution)/shard_map/all_gather | solution.py:26
  423.4 58.9 %all-to-all-start.3 = ((bf16[64,2,8192]{2,1,0:T(2,128)(2,1)}), bf16[64,2,8192]{2,1,0:T(2,128)(2,1)S(1)}, u32[]{:S(2)}, u32[]{:S(2)}) async-start(bf16[64,2,8192]{2,1,0:T(2,128)(2,1)} %reshape.559), calls=%async_computation.3 | async-start | bytes 4194304 | tf_op jit(solution)/shard_map/all_to_all | solution.py:250
  492.6 10.1 %copy-start.1 = (bf16[1,256,2048]{2,1,0:T(8,128)(2,1)S(1)}, bf16[1,256,2048]{2,1,0:T(8,128)(2,1)}, u32[]{:S(2)}) copy-start(bf16[1,256,2048]{2,1,0:T(8,128)(2,1)} %param.28) | copy-start | bytes 3145732
Sparse Core Ops, SparseCore 0:
  72.6 102.6 all-gather.3
  305.4 16.9 all-gather.5
where the time goes:
time: 518 us; the launch traced here: 510 us
  waiting for transfers between devices  274 us (53%)
  local copies, waits for them, and re-layouts  91.8 us (18%)
  matrix products  48.7 us (9%)
  other arithmetic  46.1 us (9%)
  starting transfers between devices  34.2 us (7%)
  between operations  15 us (3%)
    all_to_all x1, waiting for transfers between devices, experts_half(): arrived = lax.all_to_all(send, EP, split_axis=0, concat_axis=1, tiled=True)  189 us
    all_to_all x2, waiting for transfers between devices, sent_and_summed(): lax.all_to_all(pieces, axis, split_axis=0, concat_axis=0, tiled=True)  47.6 us
    unnamed x37, local copies, waits for them, and re-layouts  23.1 us
    all_gather x2, waiting for transfers between devices, stacked_from(): pieces = lax.all_gather(pieces, axes[k])  16.3 us
    all_to_all x1, waiting for transfers between devices, copy_for_each(): lax.all_to_all(jnp.broadcast_to(array[None], (count, *array.shape)), axis...  13.7 us
    unnamed x5, other arithmetic  13.2 us
    dot_general x8, matrix products, one_span(): jnp.einsum('hrs,shd->hrd', weights.astype(jnp.bfloat16), values_span, pre...  12.5 us
    all_to_all x1, starting transfers between devices, experts_half(): arrived = lax.all_to_all(send, EP, split_axis=0, concat_axis=1, tiled=True)  12.3 us
  transfers between devices with their start and end apart: 7, of which 5 were waited for; matrix products, arithmetic and copies ran while one was open for 24% of the time, Pallas kernels for 0%

commit v1 on v0

v1 whole, which is shorter than its diff:
```python
import functools

import jax
import jax.numpy as jnp
from jax import lax
from jax.experimental import pallas as pl
from jax.experimental.pallas import tpu as pltpu
from jax.sharding import Mesh
from jax.sharding import PartitionSpec as P

GRID_W = 64
EP = ("ep_0", "ep_1", "ep_2")
EP_TP = ("ep_0", "ep_1", "ep_2", "tp")


epsilon = 1e-06
rotary_base = 10000.0
routed_scale = 2.5


def copy_for_each(array, axis):
    count = lax.axis_size(axis)
    return lax.all_to_all(
        jnp.broadcast_to(array[None], (count, *array.shape)), axis, 0, 0, tiled=True
    )


def rotate_heads(heads_in, gain_row, positions):
    values32 = heads_in.astype(jnp.float32)
    scaled = (
        values32
        * lax.rsqrt(jnp.mean(values32 * values32, axis=-1, keepdims=True) + epsilon)
        * gain_row
    )
    pair_count = scaled.shape[-1] // 4
    inv_freq = rotary_base ** (-jnp.arange(pair_count, dtype=jnp.float32) / pair_count)
    grid_row = (positions // GRID_W).astype(jnp.float32)
    grid_col = (positions % GRID_W).astype(jnp.float32)
    angles = jnp.concatenate([grid_row[:, None] * inv_freq, grid_col[:, None] * inv_freq], axis=-1)[
        :, None, :
    ]
    cosine = jnp.cos(angles)
    sine_part = jnp.sin(angles)
    first_half = scaled[..., 0::2]
    second_half = scaled[..., 1::2]
    turned = jnp.stack(
        [
            first_half * cosine - second_half * sine_part,
            first_half * sine_part + second_half * cosine,
        ],
        axis=-1,
    )
    return turned.reshape(scaled.shape).astype(jnp.bfloat16)


def flash_kernel(q_ref, kv_ref, out_ref, max_ref, sum_ref, acc_ref, *, scale, rows):
    step = pl.program_id(0)

    @pl.when(step == 0)
    def _():
        max_ref[...] = jnp.full(max_ref.shape, -jnp.inf, jnp.float32)
        sum_ref[...] = jnp.zeros(sum_ref.shape, jnp.float32)
        acc_ref[...] = jnp.zeros(acc_ref.shape, jnp.float32)

    kv = kv_ref[...]
    for part in range(q_ref.shape[0] // rows):
        at = pl.ds(part * rows, rows)
        scores = (
            lax.dot_general(
                q_ref[at, :], kv, (((1,), (1,)), ((), ())), preferred_element_type=jnp.float32
            )
            * scale
        )
        old_max = max_ref[at, :]
        new_max = jnp.maximum(old_max, jnp.max(scores, axis=1, keepdims=True))
        factor = jnp.exp(old_max - new_max)
        weights = jnp.exp(scores - new_max)
        sum_ref[at, :] = sum_ref[at, :] * factor + jnp.sum(weights, axis=1, keepdims=True)
        acc_ref[at, :] = acc_ref[at, :] * factor + jnp.dot(
            weights.astype(jnp.bfloat16), kv, preferred_element_type=jnp.float32
        )
        max_ref[at, :] = new_max

    @pl.when(step == pl.num_programs(0) - 1)
    def _():
        out_ref[...] = (acc_ref[...] / sum_ref[...]).astype(jnp.bfloat16)


def flash(q_padded, key_value, head_size, span, rows):
    query_count, width = q_padded.shape
    key_count = key_value.shape[0]
    return pl.pallas_call(
        functools.partial(flash_kernel, scale=head_size ** (-0.5), rows=rows),
        grid=(key_count // span,),
        in_specs=[
            pl.BlockSpec((query_count, width), lambda i: (0, 0)),
            pl.BlockSpec((span, width), lambda i: (i, 0)),
        ],
        out_specs=pl.BlockSpec((query_count, width), lambda i: (0, 0)),
        out_shape=jax.ShapeDtypeStruct((query_count, width), jnp.bfloat16),
        scratch_shapes=[
            pltpu.VMEM((query_count, 1), jnp.float32),
            pltpu.VMEM((query_count, 1), jnp.float32),
            pltpu.VMEM((query_count, width), jnp.float32),
        ],
        compiler_params=pltpu.CompilerParams(dimension_semantics=("arbitrary",)),
        cost_estimate=pl.CostEstimate(
            flops=8 * query_count * key_count * width,
            bytes_accessed=2 * key_count * width,
            transcendentals=query_count * key_count,
        ),
        name="flash",
    )(q_padded, key_value)


def attend(query_rows, key_rows, value_rows, query_gain, key_gain):
    row_count = query_rows.shape[0]
    head_size = query_gain.shape[0]
    group = query_rows.shape[1] // head_size
    positions = lax.axis_index(EP) * row_count + jnp.arange(row_count, dtype=jnp.int32)
    k_rot = rotate_heads(key_rows.reshape(row_count, 1, head_size), key_gain, positions)
    key_value = jnp.concatenate([k_rot.reshape(row_count, head_size), value_rows], axis=1)
    for axis in ("ep_0", "ep_1", "ep_2"):
        with jax.named_scope("kv_" + axis):
            key_value = copy_for_each(key_value, axis)
    key_value = key_value.reshape(-1, 2 * head_size)
    q_rot = rotate_heads(query_rows.reshape(row_count, group, head_size), query_gain, positions)
    q_padded = jnp.concatenate([q_rot, jnp.zeros_like(q_rot)], axis=-1).transpose(1, 0, 2)
    q_padded = q_padded.reshape(group * row_count, 2 * head_size)
    result = flash(q_padded, key_value, head_size, 2048, 256)
    result = result[:, head_size:].reshape(group, row_count, head_size).transpose(1, 0, 2)
    return result.reshape(row_count, group * head_size)


def slots_of(routes, experts, capacity):
    tokens, top_count = routes.shape
    expert_ids = lax.broadcasted_iota(jnp.int32, (tokens, experts), 1)
    named = [(routes[:, k : k + 1] == expert_ids).astype(jnp.float32) for k in range(top_count)]
    earlier = (
        lax.broadcasted_iota(jnp.int32, (tokens, tokens), 1)
        < lax.broadcasted_iota(jnp.int32, (tokens, tokens), 0)
    ).astype(jnp.bfloat16)
    before = jnp.dot(
        earlier, sum(named).astype(jnp.bfloat16), preferred_element_type=jnp.float32
    )
    slot_ids = lax.broadcasted_iota(jnp.int32, (tokens, experts * capacity), 1)
    result = []
    for k in range(top_count):
        rank = jnp.sum(before * named[k], axis=1, keepdims=True).astype(jnp.int32)
        slot = routes[:, k : k + 1] * capacity + rank
        result.append((slot == slot_ids).astype(jnp.float32))
    return result


def dispatch_kernel(tokens_ref, gain_ref, routes_ref, send_ref, normed_ref, *, experts, capacity):
    values32 = tokens_ref[...].astype(jnp.float32)
    normed = (
        values32
        * lax.rsqrt(jnp.mean(values32 * values32, axis=-1, keepdims=True) + epsilon)
        * gain_ref[...]
    ).astype(jnp.bfloat16)
    normed_ref[...] = normed
    chosen = sum(slots_of(routes_ref[...], experts, capacity)).T.astype(jnp.bfloat16)
    send_ref[...] = jnp.dot(chosen, normed, preferred_element_type=jnp.float32).astype(
        jnp.bfloat16
    )


def combine_kernel(
    routes_ref, weights_ref, returned_ref, shared_ref, out_ref, *, experts, capacity
):
    weights = weights_ref[...]
    gates = weights / jnp.sum(weights, axis=-1, keepdims=True) * routed_scale
    returned = returned_ref[...]
    total = jnp.zeros(out_ref.shape, jnp.float32)
    for k, chosen in enumerate(slots_of(routes_ref[...], experts, capacity)):
        picked = jnp.dot(
            chosen.astype(jnp.bfloat16), returned, preferred_element_type=jnp.float32
        )
        total = total + gates[:, k : k + 1] * picked
    shared = shared_ref[0].astype(jnp.float32)
    for k in range(1, shared_ref.shape[0]):
        shared = shared + shared_ref[k].astype(jnp.float32)
    out_ref[...] = (total + shared).astype(jnp.bfloat16)


def shared_products(rows_in, w_gate, w_up, w_down):
    gate_proj = jnp.dot(rows_in, w_gate, preferred_element_type=jnp.float32)
    up_proj = jnp.dot(rows_in, w_up, preferred_element_type=jnp.float32)
    hidden = (jax.nn.silu(gate_proj) * up_proj).astype(jnp.bfloat16)
    return jnp.dot(hidden, w_down, preferred_element_type=jnp.float32)


def experts_half(
    moe_tokens,
    norm_gain,
    routes,
    route_weights,
    expert_gate,
    expert_up,
    expert_down,
    shared_gate,
    shared_up,
    shared_down,
):
    tok_rows, model_width = moe_tokens.shape
    top_count = routes.shape[1]
    experts = expert_gate.shape[0] * lax.axis_size(EP)
    capacity = 2 * tok_rows * top_count // experts
    slots = experts * capacity
    lane = lax.axis_index("tp")
    own_routes = lax.dynamic_slice_in_dim(routes, lane * tok_rows, tok_rows, 0)
    own_weights = lax.dynamic_slice_in_dim(route_weights, lane * tok_rows, tok_rows, 0)

    with jax.named_scope("weights"):
        gate_all = lax.all_gather(expert_gate[0], "tp")
        up_all = lax.all_gather(expert_up[0], "tp")
        down_all = lax.all_gather(expert_down[0], "tp")

    send, normed = pl.pallas_call(
        functools.partial(dispatch_kernel, experts=experts, capacity=capacity),
        out_shape=(
            jax.ShapeDtypeStruct((slots, model_width), jnp.bfloat16),
            jax.ShapeDtypeStruct((tok_rows, model_width), jnp.bfloat16),
        ),
        name="dispatch",
    )(moe_tokens, norm_gain[None], own_routes)

    with jax.named_scope("send_rows"):
        arrived = lax.all_to_all(
            send.reshape(experts, capacity, model_width), EP, 0, 0, tiled=True
        )
    arrived = arrived.reshape(slots, model_width)

    with jax.named_scope("shared_rows"):
        group_rows = copy_for_each(normed, "tp").reshape(-1, model_width)
    shared_part = shared_products(group_rows, shared_gate, shared_up, shared_down)
    with jax.named_scope("shared_back"):
        shared_parts = lax.all_to_all(
            shared_part.astype(jnp.bfloat16).reshape(-1, tok_rows, model_width),
            "tp",
            0,
            0,
            tiled=True,
        )

    gate_proj = jnp.einsum("rd,qdf->qrf", arrived, gate_all, preferred_element_type=jnp.float32)
    up_proj = jnp.einsum("rd,qdf->qrf", arrived, up_all, preferred_element_type=jnp.float32)
    hidden = (jax.nn.silu(gate_proj) * up_proj).astype(jnp.bfloat16)
    partial = jnp.einsum("qrf,qfd->qrd", hidden, down_all, preferred_element_type=jnp.float32)
    outgoing = jnp.sum(partial.astype(jnp.bfloat16).astype(jnp.float32), axis=0)
    with jax.named_scope("return_rows"):
        returned = lax.all_to_all(
            outgoing.astype(jnp.bfloat16).reshape(experts, capacity, model_width),
            EP,
            0,
            0,
            tiled=True,
        )
    return pl.pallas_call(
        functools.partial(combine_kernel, experts=experts, capacity=capacity),
        out_shape=jax.ShapeDtypeStruct((tok_rows, model_width), jnp.bfloat16),
        name="combine",
    )(own_routes, own_weights, returned.reshape(slots, model_width), shared_parts)


def body(
    query_rows,
    key_rows,
    value_rows,
    query_gain,
    key_gain,
    moe_tokens,
    norm_gain,
    routes,
    route_weights,
    expert_gate,
    expert_up,
    expert_down,
    shared_gate,
    shared_up,
    shared_down,
):
    attn_out = attend(query_rows, key_rows, value_rows, query_gain, key_gain)
    moe_out = experts_half(
        moe_tokens,
        norm_gain,
        routes,
        route_weights,
        expert_gate,
        expert_up,
        expert_down,
        shared_gate,
        shared_up,
        shared_down,
    )
    return (attn_out, moe_out)


def solution(mesh):
    finer = Mesh(mesh.devices.reshape(8, 4, 2, mesh.shape["tp"]), ("ep_0", "ep_1", "ep_2", "tp"))
    return jax.shard_map(
        body,
        mesh=finer,
        in_specs=(
            P(EP, "tp"),
            P(EP, "tp"),
            P(EP, "tp"),
            P(),
            P(),
            P(EP_TP, None),
            P(),
            P(EP, None),
            P(EP, None),
            P(EP, None, "tp"),
            P(EP, None, "tp"),
            P(EP, "tp", None),
            P(None, "tp"),
            P(None, "tp"),
            P("tp", None),
        ),
        out_specs=(P(EP, "tp"), P(EP_TP, None)),
        check_vma=False,
    )
```

time: 518 us -> 289 us (0.56); the launches traced: 510 us -> 288 us
  waiting for transfers between devices: 274 us -> 97.9 us
  local copies, waits for them, and re-layouts: 91.8 us -> 12.7 us
  blocking collectives: 0 us -> 56.7 us
  other arithmetic: 46.1 us -> 0.69 us
  Pallas kernels: 0 us -> 42.4 us
  matrix products: 48.7 us -> 28 us
    all_to_all x4 -> x3, waiting for transfers between devices: 243 us -> 59.5 us  [the longest x1 43.4 us: experts_half(): lax.all_to_all(send.reshape(experts, capacity, model_width), EP, 0, 0, ti...]
    all_to_all x0 -> x2, blocking collectives: none -> 56.7 us  [copy_for_each(): lax.all_to_all(jnp.broadcast_to(array[None], (count, *array.shape)), axis...]
    pallas_call x0 -> x3, Pallas kernels: none -> 42.4 us  [the longest x1 34.5 us: flash(): pl.pallas_call(functools.partial(flash_kernel, scale=head_size ** (-0.5),...]
    reduce_sum x14 -> x0, other arithmetic: 23.2 us -> none  [the longest x8 11.4 us: one_span(): run_sum = run_sum * factor + jnp.sum(weights, axis=-1)]
    all_to_all x1 -> x2, waiting for transfers between devices: 13.7 us -> 36.3 us  [copy_for_each(): lax.all_to_all(jnp.broadcast_to(array[None], (count, *array.shape)), axis...]
    dot_general x19 -> x3, matrix products: 40.6 us -> 20.3 us  [the longest x1 7.1 us: experts_half(): jnp.einsum('rd,qdf->qrf', arrived, gate_all, preferred_element_type=jnp.f...]
    unnamed x37 -> x20, local copies, waits for them, and re-layouts: 23.1 us -> 3.76 us
    transpose x3 -> x2, local copies, waits for them, and re-layouts: 19.7 us -> 0.99 us  [attend(): jnp.concatenate([q_rot, jnp.zeros_like(q_rot)], axis=-1).transpose(1, 0, 2)]
  transfers between devices with their start and end apart: 7 -> 8, of which waited for: 5 -> 5; matrix products, arithmetic and copies ran while one was open for 24% -> 14% of each run, Pallas kernels for 0% -> 13%
where the time goes in v1:
time: 289 us; the launch traced here: 288 us
  waiting for transfers between devices  97.9 us (34%)
  blocking collectives  56.7 us (20%)
  Pallas kernels  42.4 us (15%)
  starting transfers between devices  36 us (12%)
  matrix products  28 us (10%)
  between operations  14 us (5%)
  local copies, waits for them, and re-layouts  12.7 us (4%)
    all_to_all x2, blocking collectives, copy_for_each(): lax.all_to_all(jnp.broadcast_to(array[None], (count, *array.shape)), axis...  56.7 us
    all_to_all x1, waiting for transfers between devices, experts_half(): lax.all_to_all(send.reshape(experts, capacity, model_width), EP, 0, 0, ti...  43.4 us
    all_to_all x2, waiting for transfers between devices, copy_for_each(): lax.all_to_all(jnp.broadcast_to(array[None], (count, *array.shape)), axis...  36.3 us
    pallas_call x1, Pallas kernels, flash(): pl.pallas_call(functools.partial(flash_kernel, scale=head_size ** (-0.5),...  34.5 us
    all_to_all x2, starting transfers between devices, copy_for_each(): lax.all_to_all(jnp.broadcast_to(array[None], (count, *array.shape)), axis...  13.3 us
    all_to_all x1, waiting for transfers between devices, experts_half(): lax.all_to_all(outgoing.astype(jnp.bfloat16).reshape(experts, capacity, m...  11.6 us
    all_to_all x1, starting transfers between devices, experts_half(): lax.all_to_all(outgoing.astype(jnp.bfloat16).reshape(experts, capacity, m...  10.7 us
    all_to_all x1, starting transfers between devices, experts_half(): lax.all_to_all(send.reshape(experts, capacity, model_width), EP, 0, 0, ti...  8.15 us
  transfers between devices with their start and end apart: 8, of which 5 were waited for; matrix products, arithmetic and copies ran while one was open for 14% of the time, Pallas kernels for 13%

profile of v1, /device:TPU:2, one launch (start us, length us, event | category | flops | bytes accessed | tf_op | source)
XLA Modules:
  0.0 288.5 jit_solution(2101401781491204422)
XLA Ops:
  7.2 0.0 all-gather.6.cloned.1.call-start
  7.3 0.7 all-gather.6.cloned.1.call-update
  7.9 0.0 all-gather.4.cloned.1.call-start
  8.0 0.7 all-gather.4.cloned.1.call-update
  8.8 0.1 fusion.21
  8.9 0.1 fusion.30
  9.0 0.1 fusion.28
  9.2 0.1 copy.38
  9.4 0.9 broadcast_in_dim.10
  10.2 8.5 %all-to-all-start = ((bf16[8,256,128]{2,1,0:T(8,128)(2,1)}), bf16[8,256,128]{2,1,0:T(8,128)(2,1)S(1)}, u32[]{:S(2)}, u32[]{:S(2)}) async-start(bf16[8,256,128]{2,1,0:T(8,128)(2,1)} %broadcast_in_dim.10), calls=%async_computation | async-start | bytes 1048576 | tf_op jit(solution)/shard_map/kv_ep_0/all_to_all | solution.py:23
  18.7 0.7 constant_dynamic-slice_fusion.1
  19.4 0.7 copy.43.routes_ref
  20.1 3.6 %dispatch.1 = (bf16[512,2048]{1,0:T(8,128)(2,1)}, bf16[128,2048]{1,0:T(8,128)(2,1)}) custom-call(bf16[128,2048]{1,0:T(8,128)(2,1)} %tokens_ref.1, f32[1,2048]{1,0:T(1,128)} %bitcast.79, s32[128,2]{1,0:T(8,128)} %copy.43.routes_ref), custom_call_target="tpu_custom_call" | custom-call | tf_op jit(solution)/shard_map/dispatch/pallas_call | solution.py:220
  23.7 12.5 %all-to-all-done = bf16[8,256,128]{2,1,0:T(8,128)(2,1)S(1)} async-done(((bf16[8,256,128]{2,1,0:T(8,128)(2,1)}), bf16[8,256,128]{2,1,0:T(8,128)(2,1)S(1)}, u32[]{:S(2)}, u32[]{:S(2)}) %all-to-all-start) | async-done | bytes 524320 | tf_op jit(solution)/shard_map/kv_ep_0/all_to_all | solution.py:23
  36.2 1.3 broadcast_in_dim.14
  37.5 48.6 %all_to_all.35 = bf16[4,128,2048]{2,1,0:T(8,128)(2,1)} all-to-all(bf16[4,128,2048]{2,1,0:T(8,128)(2,1)S(1)} %broadcast_in_dim.14), channel_id=1, replica_groups=mesh['ep_0'=8,'ep_1'=4,'ep_2'=2,'tp'=4] {'tp'}, dimensions={0} | all-to-all | bytes 4194304 | tf_op jit(solution)/shard_map/shared_rows/all_to_all | solution.py:23
  86.1 1.9 broadcast_in_dim.11
  87.9 4.8 %all-to-all-start.1 = ((bf16[4,8,256,128]{3,2,1,0:T(8,128)(2,1)}), bf16[4,8,256,128]{3,2,1,0:T(8,128)(2,1)S(1)}, u32[]{:S(2)}, u32[]{:S(2)}) async-start(bf16[4,8,256,128]{3,2,1,0:T(8,128)(2,1)} %broadcast_in_dim.11), calls=%async_computation.1 | async-start | bytes 4194304 | tf_op jit(solution)/shard_map/kv_ep_1/all_to_all | solution.py:23
  92.7 0.7 all-gather.8.cloned.1.call-update
  93.5 23.8 %all-to-all-done.1 = bf16[4,8,256,128]{3,2,1,0:T(8,128)(2,1)S(1)} async-done(((bf16[4,8,256,128]{3,2,1,0:T(8,128)(2,1)}), bf16[4,8,256,128]{3,2,1,0:T(8,128)(2,1)S(1)}, u32[]{:S(2)}, u32[]{:S(2)}) %all-to-all-start.1) | async-done | bytes 2097184 | tf_op jit(solution)/shard_map/kv_ep_1/all_to_all | solution.py:23
  117.2 1.0 broadcast_in_dim.12
  118.2 8.2 %all_to_all.36 = bf16[2,4,8,256,128]{4,3,2,1,0:T(8,128)(2,1)} all-to-all(bf16[2,4,8,256,128]{4,3,2,1,0:T(8,128)(2,1)S(1)} %broadcast_in_dim.12), channel_id=1, replica_groups=mesh['ep_0'=8,'ep_1'=4,'ep_2'=2,'tp'=4] {'ep_2'}, dimensions={0} | all-to-all | bytes 8388608 | tf_op jit(solution)/shard_map/kv_ep_2/all_to_all | solution.py:23
  126.4 8.1 %all-to-all-start.3 = ((bf16[64,8,2048]{2,1,0:T(8,128)(2,1)}), bf16[64,8,2048]{2,1,0:T(8,128)(2,1)}, u32[]{:S(2)}, u32[]{:S(2)}) async-start(bf16[64,8,2048]{2,1,0:T(8,128)(2,1)} %bitcast.17), calls=%async_computation.3 | async-start | bytes 4194304 | tf_op jit(solution)/shard_map/send_rows/all_to_all | solution.py:230
  134.6 2.7 fusion.36
  137.3 5.0 %convolution_convert_fusion = bf16[512,2048]{1,0:T(8,128)(2,1)} fusion(bf16[256,2048]{1,0:T(8,128)(2,1)S(1)} %copy-done, bf16[512,2048]{1,0:T(8,128)(2,1)S(1)} %bitcast.73, bf16[2048,256]{1,0:T(8,128)(2,1)} %param.28, f32[512,256]{1,0:T(8,128)} %fusion.36), kind=kOutput, calls=%fused_computation.1 | convolution fusion | flops 1075576832 | bytes 6815744 | tf_op jit(solution)/shard_map/dot_general | solution.py:191
  142.3 43.4 %all-to-all-done.3 = bf16[64,8,2048]{2,1,0:T(8,128)(2,1)} async-done(((bf16[64,8,2048]{2,1,0:T(8,128)(2,1)}), bf16[64,8,2048]{2,1,0:T(8,128)(2,1)}, u32[]{:S(2)}, u32[]{:S(2)}) %all-to-all-start.3) | async-done | bytes 2097184 | tf_op jit(solution)/shard_map/send_rows/all_to_all | solution.py:230
  185.7 3.8 %all-to-all-start.6 = ((bf16[4,128,2048]{2,1,0:T(8,128)(2,1)}), bf16[4,128,2048]{2,1,0:T(8,128)(2,1)S(1)}, u32[]{:S(2)}, u32[]{:S(2)}) async-start(bf16[4,128,2048]{2,1,0:T(8,128)(2,1)} %bitcast.74), calls=%async_computation.6 | async-start | bytes 4194304 | tf_op jit(solution)/shard_map/shared_back/all_to_all | solution.py:239
  189.5 0.0 all-gather.6.cloned.1.call-done
  189.5 6.5 %fusion.1 = f32[512,4,256]{2,0,1:T(8,128)} fusion(bf16[4,2048,256]{2,1,0:T(8,128)(2,1)} %all-gather.6.cloned.1.call-done, bf16[64,8,2048]{2,1,0:T(8,128)(2,1)} %all-to-all-done.3), kind=kOutput, calls=%fused_computation.4 | convolution fusion | flops 2147483648 | bytes 8388608 | tf_op jit(solution)/shard_map/rd,qdf->qrf/dot_general | solution.py:248
  196.0 7.1 %fusion = bf16[4,512,256]{2,1,0:T(8,128)(2,1)} fusion(f32[512,4,256]{2,0,1:T(8,128)} %fusion.1, bf16[4,2048,256]{2,1,0:T(8,128)(2,1)} %all-gather.4.cloned.1.call-done, bf16[64,8,2048]{2,1,0:T(8,128)(2,1)} %all-to-all-done.3), kind=kOutput, calls=%fused_computation.3 | convolution fusion | flops 2150629376 | bytes 9437184 | tf_op jit(solution)/shard_map/rd,qdf->qrf/dot_general | solution.py:247
  203.1 6.7 %convert_reduce_fusion = bf16[512,2048]{1,0:T(8,128)(2,1)} fusion(bf16[4,512,256]{2,1,0:T(8,128)(2,1)} %fusion, bf16[4,256,2048]{2,1,0:T(8,128)(2,1)} %all-gather.8.cloned.1.call-done), kind=kOutput, calls=%fused_computation | convolution fusion | flops 2154823680 | bytes 7340032 | tf_op jit(solution)/shard_map/qrf,qfd->qrd/dot_general | solution.py:250
  209.8 4.6 %all-to-all-done.6.shared_ref = bf16[4,128,2048]{2,1,0:T(8,128)(2,1)S(1)} async-done(((bf16[4,128,2048]{2,1,0:T(8,128)(2,1)}), bf16[4,128,2048]{2,1,0:T(8,128)(2,1)S(1)}, u32[]{:S(2)}, u32[]{:S(2)}) %all-to-all-start.6) | async-done | bytes 2097184 | tf_op jit(solution)/shard_map/shared_back/all_to_all | solution.py:239
  214.4 1.4 copy-done.1
  215.8 10.7 %all-to-all-start.4 = ((bf16[64,8,2048]{2,1,0:T(8,128)(2,1)}), bf16[64,8,2048]{2,1,0:T(8,128)(2,1)}, u32[]{:S(2)}, u32[]{:S(2)}) async-start(bf16[64,8,2048]{2,1,0:T(8,128)(2,1)} %bitcast.71), calls=%async_computation.4 | async-start | bytes 4194304 | tf_op jit(solution)/shard_map/return_rows/all_to_all | solution.py:253
  226.5 0.1 copy.34
  226.7 0.1 fusion.17
  226.9 0.1 fusion.27
  227.1 0.1 copy.35
  227.2 0.1 pad_bitcast_fusion
  227.3 0.9 copy.36
  228.2 0.7 constant_dynamic-slice_fusion
  228.9 0.7 copy.44.weights_ref
  229.6 34.5 %flash.1 = bf16[1024,128]{1,0:T(8,128)(2,1)} custom-call(bf16[1024,128]{1,0:T(8,128)(2,1)} %bitcast.78, bf16[16384,128]{1,0:T(8,128)(2,1)} %bitcast.70), custom_call_target="tpu_custom_call" | custom-call | flops 17179869184 | bytes 4194304 | tf_op jit(solution)/shard_map/flash/pallas_call | solution.py:92
  264.1 1.1 slice.20
  265.2 0.1 copy.39
  265.3 0.8 copy.42
  266.1 11.6 %all-to-all-done.4 = bf16[64,8,2048]{2,1,0:T(8,128)(2,1)} async-done(((bf16[64,8,2048]{2,1,0:T(8,128)(2,1)}), bf16[64,8,2048]{2,1,0:T(8,128)(2,1)}, u32[]{:S(2)}, u32[]{:S(2)}) %all-to-all-start.4) | async-done | bytes 2097184 | tf_op jit(solution)/shard_map/return_rows/all_to_all | solution.py:253
  277.7 4.3 %combine.1 = bf16[128,2048]{1,0:T(8,128)(2,1)} custom-call(s32[128,2]{1,0:T(8,128)} %copy.43.routes_ref, f32[128,2]{1,0:T(8,128)} %copy.44.weights_ref, bf16[512,2048]{1,0:T(8,128)(2,1)} %bitcast.24.returned_ref, bf16[4,128,2048]{2,1,0:T(8,128)(2,1)} %copy-done.1), custom_call_target="tpu_custom_call" | custom-call | tf_op jit(solution)/shard_map/combine/pallas_call | solution.py:260
  (34 shorter events, 0.4 us)
Async XLA Ops:
  7.2 130.1 %copy-start = (bf16[256,2048]{1,0:T(8,128)(2,1)S(1)}, bf16[256,2048]{1,0:T(8,128)(2,1)}, u32[]{:S(2)}) copy-start(bf16[256,2048]{1,0:T(8,128)(2,1)} %param.29) | copy-start | bytes 3145732
  7.2 1.5 copy-start.3
  7.2 1.6 copy-start.6
  7.2 2.0 copy-start.5
  7.2 182.3 %all-gather.6.cloned.1.call-start = ((), (), s32[]{:S(2)}) async-start(), calls=%async_computation.8 | async-start | bytes 5242880 | tf_op jit(solution)/shard_map/weights/all_gather | solution.py:217
  7.9 188.1 %all-gather.4.cloned.1.call-start = ((), (), s32[]{:S(2)}) async-start(), calls=%async_computation.7 | async-start | bytes 5242880 | tf_op jit(solution)/shard_map/weights/all_gather | solution.py:216
  10.2 26.0 %all-to-all-start = ((bf16[8,256,128]{2,1,0:T(8,128)(2,1)}), bf16[8,256,128]{2,1,0:T(8,128)(2,1)S(1)}, u32[]{:S(2)}, u32[]{:S(2)}) async-start(bf16[8,256,128]{2,1,0:T(8,128)(2,1)} %broadcast_in_dim.10), calls=%async_computation | async-start | bytes 1048576 | tf_op jit(solution)/shard_map/kv_ep_0/all_to_all | solution.py:23
  87.9 29.3 %all-to-all-start.1 = ((bf16[4,8,256,128]{3,2,1,0:T(8,128)(2,1)}), bf16[4,8,256,128]{3,2,1,0:T(8,128)(2,1)S(1)}, u32[]{:S(2)}, u32[]{:S(2)}) async-start(bf16[4,8,256,128]{3,2,1,0:T(8,128)(2,1)} %broadcast_in_dim.11), calls=%async_computation.1 | async-start | bytes 4194304 | tf_op jit(solution)/shard_map/kv_ep_1/all_to_all | solution.py:23
  92.7 110.4 %all-gather.8.cloned.1.call-start = ((), (), s32[]{:S(2)}) async-start(), calls=%async_computation.9 | async-start | bytes 5242880 | tf_op jit(solution)/shard_map/weights/all_gather | solution.py:218
  126.4 8.2 %copy-start.2 = (bf16[4,128,2048]{2,1,0:T(8,128)(2,1)S(1)}, bf16[4,128,2048]{2,1,0:T(8,128)(2,1)}, u32[]{:S(2)}) copy-start(bf16[4,128,2048]{2,1,0:T(8,128)(2,1)} %all_to_all.35) | copy-start | bytes 6291460
  126.4 59.3 %all-to-all-start.3 = ((bf16[64,8,2048]{2,1,0:T(8,128)(2,1)}), bf16[64,8,2048]{2,1,0:T(8,128)(2,1)}, u32[]{:S(2)}, u32[]{:S(2)}) async-start(bf16[64,8,2048]{2,1,0:T(8,128)(2,1)} %bitcast.17), calls=%async_computation.3 | async-start | bytes 4194304 | tf_op jit(solution)/shard_map/send_rows/all_to_all | solution.py:230
  185.7 28.7 %all-to-all-start.6 = ((bf16[4,128,2048]{2,1,0:T(8,128)(2,1)}), bf16[4,128,2048]{2,1,0:T(8,128)(2,1)S(1)}, u32[]{:S(2)}, u32[]{:S(2)}) async-start(bf16[4,128,2048]{2,1,0:T(8,128)(2,1)} %bitcast.74), calls=%async_computation.6 | async-start | bytes 4194304 | tf_op jit(solution)/shard_map/shared_back/all_to_all | solution.py:239
  214.4 1.4 copy-start.1
  214.4 12.1 %copy-start.4 = (bf16[256,256]{1,0:T(8,128)(2,1)S(1)}, bf16[256,256]{1,0:T(8,128)(2,1)}, u32[]{:S(2)}) copy-start(bf16[256,256]{1,0:T(8,128)(2,1)} %param.15) | copy-start | bytes 393220
  214.4 12.3 %copy-start.7 = (f32[64]{0:T(128)S(1)}, f32[64]{0:T(128)}, u32[]{:S(2)}) copy-start(f32[64]{0:T(128)} %param.18) | copy-start | bytes 772
  215.8 61.9 %all-to-all-start.4 = ((bf16[64,8,2048]{2,1,0:T(8,128)(2,1)}), bf16[64,8,2048]{2,1,0:T(8,128)(2,1)}, u32[]{:S(2)}, u32[]{:S(2)}) async-start(bf16[64,8,2048]{2,1,0:T(8,128)(2,1)} %bitcast.71), calls=%async_computation.4 | async-start | bytes 4194304 | tf_op jit(solution)/shard_map/return_rows/all_to_all | solution.py:253
Sparse Core Ops, SparseCore 0:
  9.8 75.5 all-gather.5
  87.2 51.7 all-gather.3
  140.8 51.1 all-gather.7

commit v2 on v1

v2 whole, which is shorter than its diff:
```python
import functools
import math

import jax
import jax.numpy as jnp
from jax import lax
from jax.experimental import pallas as pl
from jax.sharding import Mesh
from jax.sharding import PartitionSpec as P


GRID_W = 64
EP = ("ep_0", "ep_1", "ep_2")
EP_TP = ("ep_0", "ep_1", "ep_2", "tp")


epsilon = 1e-06
rotary_base = 10000.0
routed_scale = 2.5

PARTS = 1


def shifted(array, axis, by):
    count = lax.axis_size(axis)
    return lax.ppermute(array, axis, [(i, (i + by) % count) for i in range(count)])


def rotate_heads(heads_in, gain_row, positions):
    values32 = heads_in.astype(jnp.float32)
    scaled = (
        values32
        * lax.rsqrt(jnp.mean(values32 * values32, axis=-1, keepdims=True) + epsilon)
        * gain_row
    )
    pair_count = scaled.shape[-1] // 4
    inv_freq = rotary_base ** (-jnp.arange(pair_count, dtype=jnp.float32) / pair_count)
    grid_row = (positions // GRID_W).astype(jnp.float32)
    grid_col = (positions % GRID_W).astype(jnp.float32)
    angles = jnp.concatenate([grid_row[:, None] * inv_freq, grid_col[:, None] * inv_freq], axis=-1)[
        :, None, :
    ]
    cosine = jnp.cos(angles)
    sine_part = jnp.sin(angles)
    first_half = scaled[..., 0::2]
    second_half = scaled[..., 1::2]
    turned = jnp.stack(
        [
            first_half * cosine - second_half * sine_part,
            first_half * sine_part + second_half * cosine,
        ],
        axis=-1,
    )
    return turned.reshape(scaled.shape).astype(jnp.bfloat16)


def flash_kernel(*refs, scale, rows, pieces, first, last):
    q_ref, kv_refs, refs = refs[0], refs[1 : 1 + pieces], refs[1 + pieces :]
    if not first:
        max_in, sum_in, acc_in = refs[:3]
        refs = refs[3:]
    factor_of = scale * math.log2(math.e)

    def scores_of(at, kv_ref):
        return lax.dot_general(
            q_ref[at, :], kv_ref[...], (((1,), (1,)), ((), ())), preferred_element_type=jnp.float32
        )

    def some_rows(step, unused):
        at = pl.ds(pl.multiple_of(step * rows, rows), rows)
        if first:
            run_max = jnp.full((rows, 1), -jnp.inf, jnp.float32)
            run_sum = jnp.zeros((rows, 1), jnp.float32)
            mixed = jnp.zeros((rows, q_ref.shape[1]), jnp.float32)
        else:
            run_max, run_sum, mixed = max_in[at, :], sum_in[at, :], acc_in[at, :]
        scores = scores_of(at, kv_refs[0])
        for k, kv_ref in enumerate(kv_refs):
            later = scores_of(at, kv_refs[k + 1]) if k + 1 < pieces else None
            new_max = jnp.maximum(run_max, jnp.max(scores, axis=1, keepdims=True))
            weights = jnp.exp2((scores - new_max) * factor_of)
            factor = jnp.exp2((run_max - new_max) * factor_of)
            run_sum = run_sum * factor + jnp.sum(weights, axis=1, keepdims=True)
            mixed = mixed * factor + jnp.dot(
                weights.astype(jnp.bfloat16), kv_ref[...], preferred_element_type=jnp.float32
            )
            run_max, scores = new_max, later
        if last:
            refs[0][at, :] = (mixed / run_sum).astype(jnp.bfloat16)
        else:
            refs[0][at, :], refs[1][at, :], refs[2][at, :] = run_max, run_sum, mixed
        return unused

    lax.fori_loop(0, q_ref.shape[0] // rows, some_rows, 0)


def flash(q_padded, pieces, state, last, scale):
    query_count, width = q_padded.shape
    column = jax.ShapeDtypeStruct((query_count, 1), jnp.float32)
    if last:
        out_shape = jax.ShapeDtypeStruct((query_count, width), jnp.bfloat16)
    else:
        out_shape = (column, column, jax.ShapeDtypeStruct((query_count, width), jnp.float32))
    keys = sum(piece.shape[0] for piece in pieces)
    return pl.pallas_call(
        functools.partial(
            flash_kernel,
            scale=scale,
            rows=256,
            pieces=len(pieces),
            first=state is None,
            last=last,
        ),
        out_shape=out_shape,
        cost_estimate=pl.CostEstimate(
            flops=8 * query_count * keys * width,
            bytes_accessed=2 * keys * width,
            transcendentals=query_count * keys,
        ),
        name="flash",
    )(q_padded, *pieces, *(state or ()))


def attend(query_rows, key_rows, value_rows, query_gain, key_gain):
    row_count = query_rows.shape[0]
    head_size = query_gain.shape[0]
    group = query_rows.shape[1] // head_size
    positions = lax.axis_index(EP) * row_count + jnp.arange(row_count, dtype=jnp.int32)
    k_rot = rotate_heads(key_rows.reshape(row_count, 1, head_size), key_gain, positions)
    own = jnp.concatenate([k_rot.reshape(row_count, head_size), value_rows], axis=1)
    copies = jnp.broadcast_to(own[None], (lax.axis_size("ep_0"), *own.shape))
    column = lax.all_to_all(copies, "ep_0", 0, 0, tiled=True)
    column = column.reshape(-1, own.shape[1])
    pieces = [column]
    for by in range(1, lax.axis_size("ep_1")):
        pieces.append(shifted(column, "ep_1", by))
    peers = [shifted(piece, "ep_2", 1) for piece in pieces]
    q_rot = rotate_heads(query_rows.reshape(row_count, group, head_size), query_gain, positions)
    q_padded = jnp.concatenate([q_rot, jnp.zeros_like(q_rot)], axis=-1).transpose(1, 0, 2)
    q_padded = q_padded.reshape(group * row_count, 2 * head_size)
    scale = head_size ** (-0.5)
    state = None
    for k, some in enumerate((pieces[:2], pieces[2:], peers[:2], peers[2:])):
        state = flash(q_padded, some, state, k == 3, scale)
    result = state[:, head_size:].reshape(group, row_count, head_size).transpose(1, 0, 2)
    return result.reshape(row_count, group * head_size)


def slots_of(routes, experts, capacity):
    tokens, top_count = routes.shape
    expert_ids = lax.broadcasted_iota(jnp.int32, (tokens, experts), 1)
    named = [(routes[:, k : k + 1] == expert_ids).astype(jnp.float32) for k in range(top_count)]
    earlier = (
        lax.broadcasted_iota(jnp.int32, (tokens, tokens), 1)
        < lax.broadcasted_iota(jnp.int32, (tokens, tokens), 0)
    ).astype(jnp.bfloat16)
    before = jnp.dot(
        earlier, sum(named).astype(jnp.bfloat16), preferred_element_type=jnp.float32
    )
    slot_ids = lax.broadcasted_iota(jnp.int32, (tokens, experts * capacity), 1)
    result = []
    for k in range(top_count):
        rank = jnp.sum(before * named[k], axis=1, keepdims=True).astype(jnp.int32)
        slot = routes[:, k : k + 1] * capacity + rank
        result.append((slot == slot_ids).astype(jnp.float32))
    return result


def dispatch_kernel(tokens_ref, gain_ref, routes_ref, send_ref, normed_ref, *, experts, capacity):
    values32 = tokens_ref[...].astype(jnp.float32)
    normed = (
        values32
        * lax.rsqrt(jnp.mean(values32 * values32, axis=-1, keepdims=True) + epsilon)
        * gain_ref[...]
    ).astype(jnp.bfloat16)
    normed_ref[...] = normed
    chosen = sum(slots_of(routes_ref[...], experts, capacity)).T.astype(jnp.bfloat16)
    send_ref[...] = jnp.dot(chosen, normed, preferred_element_type=jnp.float32).astype(
        jnp.bfloat16
    )


def combine_kernel(routes_ref, weights_ref, *refs, experts, capacity):
    returned_refs, shared_refs, out_ref = refs[:PARTS], refs[PARTS:-1], refs[-1]
    weights = weights_ref[...]
    gates = weights / jnp.sum(weights, axis=-1, keepdims=True) * routed_scale
    chosen = [c.astype(jnp.bfloat16) for c in slots_of(routes_ref[...], experts, capacity)]
    at = 0
    for ref in returned_refs:
        part = pl.ds(at, ref.shape[1])
        total = shared_refs[0][:, part].astype(jnp.float32)
        for shared_ref in shared_refs[1:]:
            total = total + shared_ref[:, part].astype(jnp.float32)
        for k, matrix in enumerate(chosen):
            picked = jnp.dot(matrix, ref[...], preferred_element_type=jnp.float32)
            total = total + gates[:, k : k + 1] * picked
        out_ref[:, part] = total.astype(jnp.bfloat16)
        at += ref.shape[1]


def hidden_of(gate_proj, up_proj):
    return (gate_proj / (1.0 + jnp.exp(-gate_proj)) * up_proj).astype(jnp.bfloat16)


def split_dot(rows, refs):
    total, at = None, 0
    for ref in refs:
        part = jnp.dot(
            rows[:, at : at + ref.shape[0]], ref[...], preferred_element_type=jnp.float32
        )
        total = part if total is None else total + part
        at += ref.shape[0]
    return total


def hidden_kernel(rows_ref, *refs, blocks):
    rows = rows_ref[...]
    for k in range(blocks):
        refs[2 * blocks + k][...] = hidden_of(
            jnp.dot(rows, refs[2 * k][...], preferred_element_type=jnp.float32),
            jnp.dot(rows, refs[2 * k + 1][...], preferred_element_type=jnp.float32),
        )


def hidden_blocks(rows, matrices):
    width = matrices[0][0].shape[1]
    return pl.pallas_call(
        functools.partial(hidden_kernel, blocks=len(matrices)),
        out_shape=[jax.ShapeDtypeStruct((rows.shape[0], width), jnp.bfloat16)] * len(matrices),
        cost_estimate=pl.CostEstimate(
            flops=4 * rows.size * width * len(matrices),
            bytes_accessed=4 * rows.size,
            transcendentals=0,
        ),
        name="hidden",
    )(rows, *sum(matrices, ()))


def down_kernel(*refs, blocks):
    hidden_refs, refs = refs[:blocks], refs[blocks:]
    total, at = None, 0
    for ref in hidden_refs:
        width, weights = 0, []
        while width < ref.shape[1]:
            weights.append(refs[at])
            width += refs[at].shape[0]
            at += 1
        part = split_dot(ref[...], weights).astype(jnp.bfloat16).astype(jnp.float32)
        total = part if total is None else total + part
    refs[-1][...] = total.astype(jnp.bfloat16)


def down_blocks(hidden, w_down):
    rows, width = hidden[0].shape[0], w_down[0].shape[1]
    tile = 512
    return pl.pallas_call(
        functools.partial(down_kernel, blocks=len(hidden)),
        grid=(width // tile,),
        in_specs=[pl.BlockSpec(h.shape, lambda i: (0, 0)) for h in hidden]
        + [pl.BlockSpec((w.shape[0], tile), lambda i: (0, i)) for w in w_down],
        out_specs=pl.BlockSpec((rows, tile), lambda i: (0, i)),
        out_shape=jax.ShapeDtypeStruct((rows, width), jnp.bfloat16),
        cost_estimate=pl.CostEstimate(
            flops=2 * rows * width * hidden[0].shape[1] * len(hidden),
            bytes_accessed=4 * rows * width,
            transcendentals=0,
        ),
        name="down",
    )(*hidden, *w_down)


def shared_kernel(*refs, blocks):
    rows = jnp.concatenate([ref[...] for ref in refs[:blocks]], axis=0)
    w_gate, w_up, w_down = refs[blocks : blocks + 3]
    hidden = hidden_of(
        jnp.dot(rows, w_gate[...], preferred_element_type=jnp.float32),
        jnp.dot(rows, w_up[...], preferred_element_type=jnp.float32),
    )
    part = jnp.dot(hidden, w_down[...], preferred_element_type=jnp.float32).astype(jnp.bfloat16)
    count = refs[0].shape[0]
    for k, out_ref in enumerate(refs[blocks + 3 :]):
        out_ref[...] = part[k * count : (k + 1) * count]


def shared_blocks(rows, w_gate, w_up, w_down):
    return pl.pallas_call(
        functools.partial(shared_kernel, blocks=len(rows)),
        out_shape=tuple(jax.ShapeDtypeStruct(r.shape, jnp.bfloat16) for r in rows),
        cost_estimate=pl.CostEstimate(
            flops=6 * len(rows) * rows[0].shape[0] * w_gate.size,
            bytes_accessed=6 * w_gate.size,
            transcendentals=0,
        ),
        name="shared",
    )(*rows, w_gate, w_up, w_down)


def from_both(own):
    return shifted(own, "tp", 1), shifted(own, "tp", -1)


def experts_half(
    moe_tokens,
    norm_gain,
    routes,
    route_weights,
    expert_gate,
    expert_up,
    expert_down,
    shared_gate,
    shared_up,
    shared_down,
):
    tok_rows, model_width = moe_tokens.shape
    top_count = routes.shape[1]
    experts = expert_gate.shape[0] * lax.axis_size(EP)
    capacity = 2 * tok_rows * top_count // experts
    slots = experts * capacity
    lane = lax.axis_index("tp")
    own_routes = lax.dynamic_slice_in_dim(routes, lane * tok_rows, tok_rows, 0)
    own_weights = lax.dynamic_slice_in_dim(route_weights, lane * tok_rows, tok_rows, 0)

    gate, up, down = expert_gate[0], expert_up[0], expert_down[0]
    gate_back, gate_ahead = from_both(gate)
    up_back, up_ahead = from_both(up)
    gate_opposite = shifted(gate_back, "tp", 1)
    up_opposite = shifted(up_ahead, "tp", -1)
    half = down.shape[0] // 2
    downs = []
    for part in jnp.split(down, PARTS, axis=1):
        back, ahead = from_both(part)
        upper = shifted(back[:half], "tp", 1)
        lower = shifted(ahead[half:], "tp", -1)
        downs.append((part, back, ahead, upper, lower))

    send, normed = pl.pallas_call(
        functools.partial(dispatch_kernel, experts=experts, capacity=capacity),
        out_shape=(
            jax.ShapeDtypeStruct((slots, model_width), jnp.bfloat16),
            jax.ShapeDtypeStruct((tok_rows, model_width), jnp.bfloat16),
        ),
        name="dispatch",
    )(moe_tokens, norm_gain[None], own_routes)

    arrived = lax.all_to_all(
        send.reshape(experts, capacity, model_width), EP, 0, 0, tiled=True
    )
    arrived = arrived.reshape(slots, model_width)

    turns = (1, -1, 2)
    group_rows = [normed] + [shifted(normed, "tp", by) for by in turns]
    own_part, *parts = shared_blocks(group_rows, shared_gate, shared_up, shared_down)
    shared_parts = [own_part] + [shifted(part, "tp", -by) for by, part in zip(turns, parts)]

    near = ((gate, up), (gate_back, up_back), (gate_ahead, up_ahead))
    hidden = hidden_blocks(arrived, near)
    hidden = hidden + hidden_blocks(arrived, ((gate_opposite, up_opposite),))
    returned = []
    for w_down in downs:
        outgoing = down_blocks(hidden, w_down)
        received = lax.all_to_all(
            outgoing.reshape(experts, capacity, -1), EP, 0, 0, tiled=True
        )
        returned.append(received.reshape(slots, -1))
    return pl.pallas_call(
        functools.partial(combine_kernel, experts=experts, capacity=capacity),
        out_shape=jax.ShapeDtypeStruct((tok_rows, model_width), jnp.bfloat16),
        name="combine",
    )(own_routes, own_weights, *returned, *shared_parts)


def body(
    query_rows,
    key_rows,
    value_rows,
    query_gain,
    key_gain,
    moe_tokens,
    norm_gain,
    routes,
    route_weights,
    expert_gate,
    expert_up,
    expert_down,
    shared_gate,
    shared_up,
    shared_down,
):
    attn_out = attend(query_rows, key_rows, value_rows, query_gain, key_gain)
    moe_out = experts_half(
        moe_tokens,
        norm_gain,
        routes,
        route_weights,
        expert_gate,
        expert_up,
        expert_down,
        shared_gate,
        shared_up,
        shared_down,
    )
    return (attn_out, moe_out)


def solution(mesh):
    finer = Mesh(mesh.devices.reshape(8, 4, 2, mesh.shape["tp"]), ("ep_0", "ep_1", "ep_2", "tp"))
    return jax.shard_map(
        body,
        mesh=finer,
        in_specs=(
            P(EP, "tp"),
            P(EP, "tp"),
            P(EP, "tp"),
            P(),
            P(),
            P(EP_TP, None),
            P(),
            P(EP, None),
            P(EP, None),
            P(EP, None, "tp"),
            P(EP, None, "tp"),
            P(EP, "tp", None),
            P(None, "tp"),
            P(None, "tp"),
            P("tp", None),
        ),
        out_specs=(P(EP, "tp"), P(EP_TP, None)),
        check_vma=False,
    )
```

time: 289 us -> 244 us (0.84)
  the two profiles are of different devices: /device:TPU:2 before, /device:TPU:129 now
where the time goes in v2:
time: 244 us; the launch traced here: 243 us
  waiting for transfers between devices  88.5 us (36%)
  starting transfers between devices  71 us (29%)
  Pallas kernels  68.6 us (28%)
  local copies, waits for them, and re-layouts  13.2 us (5%)
    ppermute x23, waiting for transfers between devices, shifted(): lax.ppermute(array, axis, [(i, (i + by) % count) for i in range(count)])  88.5 us
    ppermute x23, starting transfers between devices, shifted(): lax.ppermute(array, axis, [(i, (i + by) % count) for i in range(count)])  41.3 us
    pallas_call x4, Pallas kernels, flash(): pl.pallas_call(functools.partial(flash_kernel, scale=scale, rows=256, pie...  37 us
    all_to_all x1, starting transfers between devices, experts_half(): lax.all_to_all(outgoing.reshape(experts, capacity, -1), EP, 0, 0, tiled=T...  12.3 us
    pallas_call x2, Pallas kernels, hidden_blocks(): pl.pallas_call(functools.partial(hidden_kernel, blocks=len(matrices)), ou...  11.7 us
    all_to_all x1, starting transfers between devices, experts_half(): lax.all_to_all(send.reshape(experts, capacity, model_width), EP, 0, 0, ti...  10.8 us
    all_to_all x1, starting transfers between devices, attend(): column = lax.all_to_all(copies, 'ep_0', 0, 0, tiled=True)  6.65 us
    pallas_call x1, Pallas kernels, down_blocks(): pl.pallas_call(functools.partial(down_kernel, blocks=len(hidden)), grid=(...  6.61 us
  transfers between devices with their start and end apart: 26, of which 6 were waited for; matrix products, arithmetic and copies ran while one was open for 4% of the time, Pallas kernels for 25%

profile of v2, /device:TPU:129, one launch (start us, length us, event | category | flops | bytes accessed | tf_op | source)
XLA Modules:
  0.0 242.9 jit_solution(1853998091850668043)
XLA Ops:
  0.7 0.7 copy-done
  1.3 0.7 copy.34.routes_ref
  2.1 3.6 %dispatch.1 = (bf16[512,2048]{1,0:T(8,128)(2,1)}, bf16[128,2048]{1,0:T(8,128)(2,1)}) custom-call(bf16[128,2048]{1,0:T(8,128)(2,1)} %tokens_ref.1, f32[1,2048]{1,0:T(1,128)} %bitcast.49, s32[128,2]{1,0:T(8,128)} %copy.34.routes_ref), custom_call_target="tpu_custom_call" | custom-call | tf_op jit(solution)/shard_map/dispatch/pallas_call | solution.py:336
  5.7 10.8 %all-to-all-start.1 = ((bf16[64,8,2048]{2,1,0:T(8,128)(2,1)}), bf16[64,8,2048]{2,1,0:T(8,128)(2,1)S(1)}, u32[]{:S(2)}, u32[]{:S(2)}) async-start(bf16[64,8,2048]{2,1,0:T(8,128)(2,1)} %bitcast.41), calls=%async_computation.1 | async-start | bytes 4194304 | tf_op jit(solution)/shard_map/all_to_all | solution.py:345
  16.4 1.4 collective-permute-start.7
  17.8 1.5 collective-permute-start.10
  19.3 1.2 collective-permute-start.8
  20.6 1.5 collective-permute-start.14
  22.2 20.3 %collective-permute-done.7.refs_2_ = bf16[2048,256]{1,0:T(8,128)(2,1)} collective-permute-done((bf16[2048,256]{1,0:T(8,128)(2,1)}, bf16[2048,256]{1,0:T(8,128)(2,1)}, u32[]{:S(2)}, u32[]{:S(2)}) %collective-permute-start.7) | collective-permute-done | bytes 1048608 | tf_op jit(solution)/shard_map/ppermute | solution.py:26
  42.5 2.8 %collective-permute-start.12 = (bf16[2048,256]{1,0:T(8,128)(2,1)}, bf16[2048,256]{1,0:T(8,128)(2,1)}, u32[]{:S(2)}, u32[]{:S(2)}) collective-permute-start(bf16[2048,256]{1,0:T(8,128)(2,1)} %collective-permute-done.10.refs_5_), channel_id=1, source_target_pairs={{0,3},{1,0},{2,1},{3,2},{4,7},{5,4},{6,5},{7,6},{8,11},{9,8},{10,9... | collective-permute-start | bytes 3145736 | tf_op jit(solution)/shard_map/ppermute | solution.py:26
  45.3 19.7 %collective-permute-done.13.refs_5_ = bf16[256,2048]{1,0:T(8,128)(2,1)} collective-permute-done((bf16[256,2048]{1,0:T(8,128)(2,1)}, bf16[256,2048]{1,0:T(8,128)(2,1)}, u32[]{:S(2)}, u32[]{:S(2)}) %collective-permute-start.13) | collective-permute-done | bytes 1048608 | tf_op jit(solution)/shard_map/ppermute | solution.py:26
  65.0 1.4 collective-permute-start.9
  66.8 0.9 broadcast_in_dim.4
  67.8 6.6 %all-to-all-start = ((bf16[8,256,128]{2,1,0:T(8,128)(2,1)}), bf16[8,256,128]{2,1,0:T(8,128)(2,1)}, u32[]{:S(2)}, u32[]{:S(2)}) async-start(bf16[8,256,128]{2,1,0:T(8,128)(2,1)} %broadcast_in_dim.4), calls=%async_computation | async-start | bytes 1048576 | tf_op jit(solution)/shard_map/all_to_all | solution.py:132
  74.4 1.9 slice.29
  76.4 1.9 slice.30
  78.3 31.5 %collective-permute-done.11.refs_0_ = bf16[2048,256]{1,0:T(8,128)(2,1)S(1)} collective-permute-done((bf16[2048,256]{1,0:T(8,128)(2,1)}, bf16[2048,256]{1,0:T(8,128)(2,1)S(1)}, u32[]{:S(2)}, u32[]{:S(2)}) %collective-permute-start.11) | collective-permute-done | bytes 1048608 | tf_op jit(solution)/shard_map/ppermute | solution.py:26
  109.8 1.5 collective-permute-start.16
  111.3 4.2 %hidden.3.refs_3_ = bf16[512,256]{1,0:T(8,128)(2,1)} custom-call(bf16[512,2048]{1,0:T(8,128)(2,1)} %bitcast.38, bf16[2048,256]{1,0:T(8,128)(2,1)} %copy-done.3, bf16[2048,256]{1,0:T(8,128)(2,1)} %collective-permute-done.12.refs_1_), custom_call_target="tpu_custom_call" | custom-call | flops 1073741824 | bytes 4194304 | tf_op jit(solution)/shard_map/hidden/pallas_call | solution.py:227
  115.5 7.6 %hidden.2 = (bf16[512,256]{1,0:T(8,128)(2,1)}, bf16[512,256]{1,0:T(8,128)(2,1)}, bf16[512,256]{1,0:T(8,128)(2,1)}) custom-call(bf16[512,2048]{1,0:T(8,128)(2,1)} %bitcast.39, bf16[2048,256]{1,0:T(8,128)(2,1)} %bitcast.19.refs_0_, bf16[2048,256]{1,0:T(8,128)(2,1)} %bitcast.20.refs_1_, bf16[2048,256]{1,0:T(8,128)(2,1)} %collective-permute-done.7.refs_2_, ...), custom_call_target="tpu_custom_call" | custom-call | flops 3221225472 | bytes 4194304 | tf_op jit(solution)/shard_map/hidden/pallas_call | solution.py:227
  123.0 6.6 %down.1 = bf16[512,2048]{1,0:T(8,128)(2,1)} custom-call(bf16[512,256]{1,0:T(8,128)(2,1)} %get-tuple-element.30.refs_0_, bf16[512,256]{1,0:T(8,128)(2,1)} %get-tuple-element.31.refs_1_, bf16[512,256]{1,0:T(8,128)(2,1)} %get-tuple-element.32.refs_2_, bf16[512,256]{1,0:T(8,128)(2,1)} %hidden.3.refs_3_, bf16[256,2048]{1,0:T(8,128)(2,1)} %bitcast.21.refs_4_, ...), custom_call_target="tpu_custom_call" | custom-call | flops 2147483648 | bytes 4194304 | tf_op jit(solution)/shard_map/down/pallas_call | solution.py:256
  129.7 12.3 %all-to-all-start.2 = ((bf16[64,8,2048]{2,1,0:T(8,128)(2,1)}), bf16[64,8,2048]{2,1,0:T(8,128)(2,1)S(1)}, u32[]{:S(2)}, u32[]{:S(2)}) async-start(bf16[64,8,2048]{2,1,0:T(8,128)(2,1)} %bitcast.40), calls=%async_computation.2 | async-start | bytes 4194304 | tf_op jit(solution)/shard_map/all_to_all | solution.py:361
  142.1 2.7 %collective-permute-start.18 = (bf16[128,2048]{1,0:T(8,128)(2,1)S(1)}, bf16[128,2048]{1,0:T(8,128)(2,1)}, u32[]{:S(2)}, u32[]{:S(2)}) collective-permute-start(bf16[128,2048]{1,0:T(8,128)(2,1)S(1)} %copy-done.11), channel_id=1, source_target_pairs={{0,3},{1,0},{2,1},{3,2},{4,7},{5,4},{6,5},{7,6},{8,11},{9,8},{10,9... | collective-permute-start | bytes 1572872 | tf_op jit(solution)/shard_map/ppermute | solution.py:26
  145.5 0.7 constant_dynamic-slice_fusion
  146.3 0.7 copy.35.weights_ref
  147.0 1.2 collective-permute-start.5
  148.5 0.9 copy.27
  149.4 2.4 collective-permute-start
  151.8 4.7 %collective-permute-done.17.refs_1_ = bf16[128,2048]{1,0:T(8,128)(2,1)} collective-permute-done((bf16[128,2048]{1,0:T(8,128)(2,1)S(1)}, bf16[128,2048]{1,0:T(8,128)(2,1)}, u32[]{:S(2)}, u32[]{:S(2)}) %collective-permute-start.17) | collective-permute-done | bytes 524320 | tf_op jit(solution)/shard_map/ppermute | solution.py:26
  156.5 2.4 %collective-permute-start.2 = (bf16[2048,128]{1,0:T(8,128)(2,1)}, bf16[2048,128]{1,0:T(8,128)(2,1)}, u32[]{:S(2)}, u32[]{:S(2)}) collective-permute-start(bf16[2048,128]{1,0:T(8,128)(2,1)} %bitcast.12.refs_1_), channel_id=1, source_target_pairs={{0,24},{8,0},{16,8},{24,16},{1,25},{9,1},{17,9},{25,17},{2,26},{10... | collective-permute-start | bytes 1572872 | tf_op jit(solution)/shard_map/ppermute | solution.py:26
  158.9 9.1 %collective-permute-done.19.refs_3_ = bf16[128,2048]{1,0:T(8,128)(2,1)} collective-permute-done((bf16[128,2048]{1,0:T(8,128)(2,1)S(1)}, bf16[128,2048]{1,0:T(8,128)(2,1)}, u32[]{:S(2)}, u32[]{:S(2)}) %collective-permute-start.19) | collective-permute-done | bytes 524320 | tf_op jit(solution)/shard_map/ppermute | solution.py:26
  168.1 5.5 %shared.1 = (bf16[128,2048]{1,0:T(8,128)(2,1)}, bf16[128,2048]{1,0:T(8,128)(2,1)}, bf16[128,2048]{1,0:T(8,128)(2,1)}, bf16[128,2048]{1,0:T(8,128)(2,1)}) custom-call(bf16[128,2048]{1,0:T(8,128)(2,1)} %get-tuple-element.33.refs_0_, bf16[128,2048]{1,0:T(8,128)(2,1)} %collective-permute-done.17.refs_1_, bf16[128,2048]{1,0:T(8,128)(2,1)} %collective-permute-done.18.refs_2_, ...), custom_call_target="tpu_custom_call" | custom-call | flops 1610612736 | bytes 3145728 | tf_op jit(solution)/shard_map/shared/pallas_call | solution.py:286
  173.6 2.1 collective-permute-start.20
  175.7 1.8 collective-permute-start.4
  177.5 10.2 %collective-permute-start.6 = (bf16[2048,128]{1,0:T(8,128)(2,1)}, bf16[2048,128]{1,0:T(8,128)(2,1)}, u32[]{:S(2)}, u32[]{:S(2)}) collective-permute-start(bf16[2048,128]{1,0:T(8,128)(2,1)} %collective-permute-done.5.refs_2_), channel_id=1, source_target_pairs={{0,4},{4,0},{1,5},{5,1},{2,6},{6,2},{3,7},{7,3},{8,12},{12,8},{9,1... | collective-permute-start | bytes 1572872 | tf_op jit(solution)/shard_map/ppermute | solution.py:26
  187.7 8.9 %flash.4 = (f32[1024,1]{1,0:T(8,128)}, f32[1024,1]{1,0:T(8,128)}, f32[1024,128]{1,0:T(8,128)}) custom-call(bf16[1024,128]{1,0:T(8,128)(2,1)} %bitcast.45, bf16[2048,128]{1,0:T(8,128)(2,1)} %bitcast.12.refs_1_, bf16[2048,128]{1,0:T(8,128)(2,1)} %collective-permute-done.5.refs_2_), custom_call_target="tpu_custom_call" | custom-call | flops 4294967296 | bytes 1048576 | tf_op jit(solution)/shard_map/flash/pallas_call | solution.py:105
  196.6 0.5 collective-permute-start.3
  197.1 9.5 %flash.5 = (f32[1024,1]{1,0:T(8,128)}, f32[1024,1]{1,0:T(8,128)}, f32[1024,128]{1,0:T(8,128)}) custom-call(bf16[1024,128]{1,0:T(8,128)(2,1)} %bitcast.46, bf16[2048,128]{1,0:T(8,128)(2,1)} %collective-permute-done.refs_1_, bf16[2048,128]{1,0:T(8,128)(2,1)} %collective-permute-done.2.refs_2_, f32[1024,1]{1,0:T(8,128)} %get-tuple-element.20.refs_3_, ...), custom_call_target="tpu_custom_call" | custom-call | flops 4294967296 | bytes 1048576 | tf_op jit(solution)/shard_map/flash/pallas_call | solution.py:105
  206.6 0.8 copy-done.12
  207.4 1.2 collective-permute-start.21
  208.6 5.1 %collective-permute-start.22 = (bf16[128,2048]{1,0:T(8,128)(2,1)}, bf16[128,2048]{1,0:T(8,128)(2,1)}, u32[]{:S(2)}, u32[]{:S(2)}) collective-permute-start(bf16[128,2048]{1,0:T(8,128)(2,1)} %get-tuple-element.37), channel_id=1, source_target_pairs={{0,2},{1,3},{2,0},{3,1},{4,6},{5,7},{6,4},{7,5},{8,10},{9,11},{10,... | collective-permute-start | bytes 1572872 | tf_op jit(solution)/shard_map/ppermute | solution.py:26
  213.7 9.4 %flash.6 = (f32[1024,1]{1,0:T(8,128)}, f32[1024,1]{1,0:T(8,128)}, f32[1024,128]{1,0:T(8,128)}) custom-call(bf16[1024,128]{1,0:T(8,128)(2,1)} %bitcast.47, bf16[2048,128]{1,0:T(8,128)(2,1)} %copy-done.12, bf16[2048,128]{1,0:T(8,128)(2,1)} %collective-permute-done.6.refs_2_, f32[1024,1]{1,0:T(8,128)} %get-tuple-element.23.refs_3_, ...), custom_call_target="tpu_custom_call" | custom-call | flops 4294967296 | bytes 1048576 | tf_op jit(solution)/shard_map/flash/pallas_call | solution.py:105
  223.1 9.2 %flash.7 = bf16[1024,128]{1,0:T(8,128)(2,1)} custom-call(bf16[1024,128]{1,0:T(8,128)(2,1)} %bitcast.48, bf16[2048,128]{1,0:T(8,128)(2,1)} %collective-permute-done.1.refs_1_, bf16[2048,128]{1,0:T(8,128)(2,1)} %collective-permute-done.3.refs_2_, f32[1024,1]{1,0:T(8,128)} %get-tuple-element.26.refs_3_, f32[1024,1]{1,0:T(8,128)} %get-tuple-element.27.refs_4_, ...), custom_call_target="tpu_custom_call" | custom-call | flops 4294967296 | bytes 1048576 | tf_op jit(solution)/shard_map/flash/pallas_call | solution.py:105
  232.3 1.1 slice.28
  233.6 0.8 copy.33
  234.3 3.1 %collective-permute-done.22.refs_4_ = bf16[128,2048]{1,0:T(8,128)(2,1)} collective-permute-done((bf16[128,2048]{1,0:T(8,128)(2,1)}, bf16[128,2048]{1,0:T(8,128)(2,1)}, u32[]{:S(2)}, u32[]{:S(2)}) %collective-permute-start.22) | collective-permute-done | bytes 524320 | tf_op jit(solution)/shard_map/ppermute | solution.py:26
  237.5 1.3 copy-done.1
  238.8 4.1 %combine.1 = bf16[128,2048]{1,0:T(8,128)(2,1)} custom-call(s32[128,2]{1,0:T(8,128)} %copy.34.routes_ref, f32[128,2]{1,0:T(8,128)} %copy.35.weights_ref, bf16[512,2048]{1,0:T(8,128)(2,1)} %bitcast.37, bf16[128,2048]{1,0:T(8,128)(2,1)} %get-tuple-element.34.refs_1_, bf16[128,2048]{1,0:T(8,128)(2,1)} %copy-done.4, bf16[128,2048]{1,0:T(8,128)(2,1)} %copy-done.5, ...), custom_call_target="tpu_custom_call" | custom-call | tf_op jit(solution)/shard_map/combine/pallas_call | solution.py:365
  (76 shorter events, 2.0 us)
Async XLA Ops:
  0.6 0.7 copy-start
  5.7 16.4 %copy-start.6 = (bf16[256,64]{0,1:T(8,128)(2,1)S(1)}, bf16[256,64]{0,1:T(8,128)(2,1)}, u32[]{:S(2)}) copy-start(bf16[256,64]{0,1:T(8,128)(2,1)} %param.16) | copy-start | bytes 98308
  5.7 16.4 %copy-start.9 = (f32[64]{0:T(128)S(1)}, f32[64]{0:T(128)}, u32[]{:S(2)}) copy-start(f32[64]{0:T(128)} %param.19) | copy-start | bytes 772
  5.7 61.0 %copy-start.8 = (bf16[256,64]{0,1:T(8,128)(2,1)S(1)}, bf16[256,64]{0,1:T(8,128)(2,1)}, u32[]{:S(2)}) copy-start(bf16[256,64]{0,1:T(8,128)(2,1)} %param.17) | copy-start | bytes 98308
  5.7 61.1 %all-to-all-start.1 = ((bf16[64,8,2048]{2,1,0:T(8,128)(2,1)}), bf16[64,8,2048]{2,1,0:T(8,128)(2,1)S(1)}, u32[]{:S(2)}, u32[]{:S(2)}) async-start(bf16[64,8,2048]{2,1,0:T(8,128)(2,1)} %bitcast.41), calls=%async_computation.1 | async-start | bytes 4194304 | tf_op jit(solution)/shard_map/all_to_all | solution.py:345
  16.4 26.1 %collective-permute-start.7 = (bf16[2048,256]{1,0:T(8,128)(2,1)}, bf16[2048,256]{1,0:T(8,128)(2,1)}, u32[]{:S(2)}, u32[]{:S(2)}) collective-permute-start(bf16[2048,256]{1,0:T(8,128)(2,1)} %bitcast.19.refs_0_), channel_id=1, source_target_pairs={{0,1},{1,2},{2,3},{3,0},{4,5},{5,6},{6,7},{7,4},{8,9},{9,10},{10,1... | collective-permute-start | bytes 3145736 | tf_op jit(solution)/shard_map/ppermute | solution.py:26
  17.8 24.7 %collective-permute-start.10 = (bf16[2048,256]{1,0:T(8,128)(2,1)}, bf16[2048,256]{1,0:T(8,128)(2,1)}, u32[]{:S(2)}, u32[]{:S(2)}) collective-permute-start(bf16[2048,256]{1,0:T(8,128)(2,1)} %bitcast.20.refs_1_), channel_id=1, source_target_pairs={{0,3},{1,0},{2,1},{3,2},{4,7},{5,4},{6,5},{7,6},{8,11},{9,8},{10,9... | collective-permute-start | bytes 3145736 | tf_op jit(solution)/shard_map/ppermute | solution.py:26
  19.3 45.6 %collective-permute-start.13 = (bf16[256,2048]{1,0:T(8,128)(2,1)}, bf16[256,2048]{1,0:T(8,128)(2,1)}, u32[]{:S(2)}, u32[]{:S(2)}) collective-permute-start(bf16[256,2048]{1,0:T(8,128)(2,1)} %bitcast.21.refs_4_), channel_id=1, source_target_pairs={{0,1},{1,2},{2,3},{3,0},{4,5},{5,6},{6,7},{7,4},{8,9},{9,10},{10,1... | collective-permute-start | bytes 3145736 | tf_op jit(solution)/shard_map/ppermute | solution.py:26
  19.3 96.1 %collective-permute-start.8 = (bf16[2048,256]{1,0:T(8,128)(2,1)}, bf16[2048,256]{1,0:T(8,128)(2,1)}, u32[]{:S(2)}, u32[]{:S(2)}) collective-permute-start(bf16[2048,256]{1,0:T(8,128)(2,1)} %bitcast.20.refs_1_), channel_id=1, source_target_pairs={{0,1},{1,2},{2,3},{3,0},{4,5},{5,6},{6,7},{7,4},{8,9},{9,10},{10,1... | collective-permute-start | bytes 3145736 | tf_op jit(solution)/shard_map/ppermute | solution.py:26
  20.6 55.7 %collective-permute-start.14 = (bf16[256,2048]{1,0:T(8,128)(2,1)}, bf16[256,2048]{1,0:T(8,128)(2,1)}, u32[]{:S(2)}, u32[]{:S(2)}) collective-permute-start(bf16[256,2048]{1,0:T(8,128)(2,1)} %bitcast.21.refs_4_), channel_id=1, source_target_pairs={{0,3},{1,0},{2,1},{3,2},{4,7},{5,4},{6,5},{7,6},{8,11},{9,8},{10,9... | collective-permute-start | bytes 3145736 | tf_op jit(solution)/shard_map/ppermute | solution.py:26
  42.5 67.3 %collective-permute-start.11 = (bf16[2048,256]{1,0:T(8,128)(2,1)}, bf16[2048,256]{1,0:T(8,128)(2,1)S(1)}, u32[]{:S(2)}, u32[]{:S(2)}) collective-permute-start(bf16[2048,256]{1,0:T(8,128)(2,1)} %collective-permute-done.7.refs_2_), channel_id=1, source_target_pairs={{0,1},{1,2},{2,3},{3,0},{4,5},{5,6},{6,7},{7,4},{8,9},{9,10},{10,1... | collective-permute-start | bytes 3145736 | tf_op jit(solution)/shard_map/ppermute | solution.py:26
  42.5 68.8 %collective-permute-start.12 = (bf16[2048,256]{1,0:T(8,128)(2,1)}, bf16[2048,256]{1,0:T(8,128)(2,1)}, u32[]{:S(2)}, u32[]{:S(2)}) collective-permute-start(bf16[2048,256]{1,0:T(8,128)(2,1)} %collective-permute-done.10.refs_5_), channel_id=1, source_target_pairs={{0,3},{1,0},{2,1},{3,2},{4,7},{5,4},{6,5},{7,6},{8,11},{9,8},{10,9... | collective-permute-start | bytes 3145736 | tf_op jit(solution)/shard_map/ppermute | solution.py:26
  65.0 50.5 %collective-permute-start.9 = (bf16[2048,256]{1,0:T(8,128)(2,1)}, bf16[2048,256]{1,0:T(8,128)(2,1)}, u32[]{:S(2)}, u32[]{:S(2)}) collective-permute-start(bf16[2048,256]{1,0:T(8,128)(2,1)} %bitcast.19.refs_0_), channel_id=1, source_target_pairs={{0,3},{1,0},{2,1},{3,2},{4,7},{5,4},{6,5},{7,6},{8,11},{9,8},{10,9... | collective-permute-start | bytes 3145736 | tf_op jit(solution)/shard_map/ppermute | solution.py:26
  66.8 44.5 %copy-start.2 = (bf16[64,8,2048]{2,1,0:T(8,128)(2,1)}, bf16[64,8,2048]{2,1,0:T(8,128)(2,1)S(1)}, u32[]{:S(2)}) copy-start(bf16[64,8,2048]{2,1,0:T(8,128)(2,1)S(1)} %all-to-all-done.1) | copy-start | bytes 6291460
  67.8 61.9 %all-to-all-start = ((bf16[8,256,128]{2,1,0:T(8,128)(2,1)}), bf16[8,256,128]{2,1,0:T(8,128)(2,1)}, u32[]{:S(2)}, u32[]{:S(2)}) async-start(bf16[8,256,128]{2,1,0:T(8,128)(2,1)} %broadcast_in_dim.4), calls=%async_computation | async-start | bytes 1048576 | tf_op jit(solution)/shard_map/all_to_all | solution.py:132
  76.3 46.7 %collective-permute-start.15 = (bf16[128,2048]{1,0:T(8,128)(2,1)}, bf16[128,2048]{1,0:T(8,128)(2,1)}, u32[]{:S(2)}, u32[]{:S(2)}) collective-permute-start(bf16[128,2048]{1,0:T(8,128)(2,1)} %slice.29), channel_id=1, source_target_pairs={{0,1},{1,2},{2,3},{3,0},{4,5},{5,6},{6,7},{7,4},{8,9},{9,10},{10,1... | collective-permute-start | bytes 1572872 | tf_op jit(solution)/shard_map/ppermute | solution.py:26
  109.8 1.5 copy-start.3
  109.8 13.2 %collective-permute-start.16 = (bf16[128,2048]{1,0:T(8,128)(2,1)}, bf16[128,2048]{1,0:T(8,128)(2,1)}, u32[]{:S(2)}, u32[]{:S(2)}) collective-permute-start(bf16[128,2048]{1,0:T(8,128)(2,1)} %slice.30), channel_id=1, source_target_pairs={{0,3},{1,0},{2,1},{3,2},{4,7},{5,4},{6,5},{7,6},{8,11},{9,8},{10,9... | collective-permute-start | bytes 1572872 | tf_op jit(solution)/shard_map/ppermute | solution.py:26
  129.7 12.4 %copy-start.11 = (bf16[128,2048]{1,0:T(8,128)(2,1)S(1)}, bf16[128,2048]{1,0:T(8,128)(2,1)}, u32[]{:S(2)}) copy-start(bf16[128,2048]{1,0:T(8,128)(2,1)} %get-tuple-element.33.refs_0_) | copy-start | bytes 1572868
  129.7 15.5 %copy-start.7 = (bf16[256,256]{1,0:T(8,128)(2,1)S(1)}, bf16[256,256]{1,0:T(8,128)(2,1)}, u32[]{:S(2)}) copy-start(bf16[256,256]{1,0:T(8,128)(2,1)} %param.15) | copy-start | bytes 393220
  129.7 15.8 %copy-start.10 = (f32[64]{0:T(128)S(1)}, f32[64]{0:T(128)}, u32[]{:S(2)}) copy-start(f32[64]{0:T(128)} %param.18) | copy-start | bytes 772
  129.7 107.8 %all-to-all-start.2 = ((bf16[64,8,2048]{2,1,0:T(8,128)(2,1)}), bf16[64,8,2048]{2,1,0:T(8,128)(2,1)S(1)}, u32[]{:S(2)}, u32[]{:S(2)}) async-start(bf16[64,8,2048]{2,1,0:T(8,128)(2,1)} %bitcast.40), calls=%async_computation.2 | async-start | bytes 4194304 | tf_op jit(solution)/shard_map/all_to_all | solution.py:361
  142.0 14.5 %collective-permute-start.17 = (bf16[128,2048]{1,0:T(8,128)(2,1)S(1)}, bf16[128,2048]{1,0:T(8,128)(2,1)}, u32[]{:S(2)}, u32[]{:S(2)}) collective-permute-start(bf16[128,2048]{1,0:T(8,128)(2,1)S(1)} %copy-done.11), channel_id=1, source_target_pairs={{0,1},{1,2},{2,3},{3,0},{4,5},{5,6},{6,7},{7,4},{8,9},{9,10},{10,1... | collective-permute-start | bytes 1572872 | tf_op jit(solution)/shard_map/ppermute | solution.py:26
  142.1 16.8 %collective-permute-start.18 = (bf16[128,2048]{1,0:T(8,128)(2,1)S(1)}, bf16[128,2048]{1,0:T(8,128)(2,1)}, u32[]{:S(2)}, u32[]{:S(2)}) collective-permute-start(bf16[128,2048]{1,0:T(8,128)(2,1)S(1)} %copy-done.11), channel_id=1, source_target_pairs={{0,3},{1,0},{2,1},{3,2},{4,7},{5,4},{6,5},{7,6},{8,11},{9,8},{10,9... | collective-permute-start | bytes 1572872 | tf_op jit(solution)/shard_map/ppermute | solution.py:26
  144.8 23.3 %collective-permute-start.19 = (bf16[128,2048]{1,0:T(8,128)(2,1)S(1)}, bf16[128,2048]{1,0:T(8,128)(2,1)}, u32[]{:S(2)}, u32[]{:S(2)}) collective-permute-start(bf16[128,2048]{1,0:T(8,128)(2,1)S(1)} %copy-done.11), channel_id=1, source_target_pairs={{0,2},{1,3},{2,0},{3,1},{4,6},{5,7},{6,4},{7,5},{8,10},{9,11},{10,... | collective-permute-start | bytes 1572872 | tf_op jit(solution)/shard_map/ppermute | solution.py:26
  147.0 30.4 %collective-permute-start.5 = (bf16[2048,128]{1,0:T(8,128)(2,1)}, bf16[2048,128]{1,0:T(8,128)(2,1)}, u32[]{:S(2)}, u32[]{:S(2)}) collective-permute-start(bf16[2048,128]{1,0:T(8,128)(2,1)} %bitcast.12.refs_1_), channel_id=1, source_target_pairs={{0,8},{8,16},{16,24},{24,0},{1,9},{9,17},{17,25},{25,1},{2,10},{10... | collective-permute-start | bytes 1572872 | tf_op jit(solution)/shard_map/ppermute | solution.py:26
  149.4 47.2 %collective-permute-start = (bf16[2048,128]{1,0:T(8,128)(2,1)}, bf16[2048,128]{1,0:T(8,128)(2,1)}, u32[]{:S(2)}, u32[]{:S(2)}) collective-permute-start(bf16[2048,128]{1,0:T(8,128)(2,1)} %bitcast.12.refs_1_), channel_id=1, source_target_pairs={{0,16},{8,24},{16,0},{24,8},{1,17},{9,25},{17,1},{25,9},{2,18},{10... | collective-permute-start | bytes 1572872 | tf_op jit(solution)/shard_map/ppermute | solution.py:26
  156.5 40.1 %collective-permute-start.2 = (bf16[2048,128]{1,0:T(8,128)(2,1)}, bf16[2048,128]{1,0:T(8,128)(2,1)}, u32[]{:S(2)}, u32[]{:S(2)}) collective-permute-start(bf16[2048,128]{1,0:T(8,128)(2,1)} %bitcast.12.refs_1_), channel_id=1, source_target_pairs={{0,24},{8,0},{16,8},{24,16},{1,25},{9,1},{17,9},{25,17},{2,26},{10... | collective-permute-start | bytes 1572872 | tf_op jit(solution)/shard_map/ppermute | solution.py:26
  173.6 60.7 %collective-permute-start.20 = (bf16[128,2048]{1,0:T(8,128)(2,1)}, bf16[128,2048]{1,0:T(8,128)(2,1)S(1)}, u32[]{:S(2)}, u32[]{:S(2)}) collective-permute-start(bf16[128,2048]{1,0:T(8,128)(2,1)} %get-tuple-element.35), channel_id=1, source_target_pairs={{0,3},{1,0},{2,1},{3,2},{4,7},{5,4},{6,5},{7,6},{8,11},{9,8},{10,9... | collective-permute-start | bytes 1572872 | tf_op jit(solution)/shard_map/ppermute | solution.py:26
  175.7 31.0 %collective-permute-start.4 = (bf16[2048,128]{1,0:T(8,128)(2,1)}, bf16[2048,128]{1,0:T(8,128)(2,1)S(1)}, u32[]{:S(2)}, u32[]{:S(2)}) collective-permute-start(bf16[2048,128]{1,0:T(8,128)(2,1)} %bitcast.12.refs_1_), channel_id=1, source_target_pairs={{0,4},{4,0},{1,5},{5,1},{2,6},{6,2},{3,7},{7,3},{8,12},{12,8},{9,1... | collective-permute-start | bytes 1572872 | tf_op jit(solution)/shard_map/ppermute | solution.py:26
  177.5 31.1 %collective-permute-start.6 = (bf16[2048,128]{1,0:T(8,128)(2,1)}, bf16[2048,128]{1,0:T(8,128)(2,1)}, u32[]{:S(2)}, u32[]{:S(2)}) collective-permute-start(bf16[2048,128]{1,0:T(8,128)(2,1)} %collective-permute-done.5.refs_2_), channel_id=1, source_target_pairs={{0,4},{4,0},{1,5},{5,1},{2,6},{6,2},{3,7},{7,3},{8,12},{12,8},{9,1... | collective-permute-start | bytes 1572872 | tf_op jit(solution)/shard_map/ppermute | solution.py:26
  196.6 26.5 %collective-permute-start.1 = (bf16[2048,128]{1,0:T(8,128)(2,1)}, bf16[2048,128]{1,0:T(8,128)(2,1)}, u32[]{:S(2)}, u32[]{:S(2)}) collective-permute-start(bf16[2048,128]{1,0:T(8,128)(2,1)} %collective-permute-done.refs_1_), channel_id=1, source_target_pairs={{0,4},{4,0},{1,5},{5,1},{2,6},{6,2},{3,7},{7,3},{8,12},{12,8},{9,1... | collective-permute-start | bytes 1572872 | tf_op jit(solution)/shard_map/ppermute | solution.py:26
  196.6 26.5 %collective-permute-start.3 = (bf16[2048,128]{1,0:T(8,128)(2,1)}, bf16[2048,128]{1,0:T(8,128)(2,1)}, u32[]{:S(2)}, u32[]{:S(2)}) collective-permute-start(bf16[2048,128]{1,0:T(8,128)(2,1)} %collective-permute-done.2.refs_2_), channel_id=1, source_target_pairs={{0,4},{4,0},{1,5},{5,1},{2,6},{6,2},{3,7},{7,3},{8,12},{12,8},{9,1... | collective-permute-start | bytes 1572872 | tf_op jit(solution)/shard_map/ppermute | solution.py:26
  206.6 0.8 copy-start.12
  207.4 26.9 %collective-permute-start.21 = (bf16[128,2048]{1,0:T(8,128)(2,1)}, bf16[128,2048]{1,0:T(8,128)(2,1)S(1)}, u32[]{:S(2)}, u32[]{:S(2)}) collective-permute-start(bf16[128,2048]{1,0:T(8,128)(2,1)} %get-tuple-element.36), channel_id=1, source_target_pairs={{0,1},{1,2},{2,3},{3,0},{4,5},{5,6},{6,7},{7,4},{8,9},{9,10},{10,1... | collective-permute-start | bytes 1572872 | tf_op jit(solution)/shard_map/ppermute | solution.py:26
  208.6 28.8 %collective-permute-start.22 = (bf16[128,2048]{1,0:T(8,128)(2,1)}, bf16[128,2048]{1,0:T(8,128)(2,1)}, u32[]{:S(2)}, u32[]{:S(2)}) collective-permute-start(bf16[128,2048]{1,0:T(8,128)(2,1)} %get-tuple-element.37), channel_id=1, source_target_pairs={{0,2},{1,3},{2,0},{3,1},{4,6},{5,7},{6,4},{7,5},{8,10},{9,11},{10,... | collective-permute-start | bytes 1572872 | tf_op jit(solution)/shard_map/ppermute | solution.py:26
  234.3 3.1 %copy-start.4 = (bf16[128,2048]{1,0:T(8,128)(2,1)}, bf16[128,2048]{1,0:T(8,128)(2,1)S(1)}, u32[]{:S(2)}) copy-start(bf16[128,2048]{1,0:T(8,128)(2,1)S(1)} %collective-permute-done.20.refs_2_) | copy-start | bytes 1572868
  234.3 3.1 %copy-start.5 = (bf16[128,2048]{1,0:T(8,128)(2,1)}, bf16[128,2048]{1,0:T(8,128)(2,1)S(1)}, u32[]{:S(2)}) copy-start(bf16[128,2048]{1,0:T(8,128)(2,1)S(1)} %collective-permute-done.21.refs_3_) | copy-start | bytes 1572868
  237.4 1.3 copy-start.1
